TPU v7x, 512 devices: a 8x2x16 block of a 8x16x16 slice. The times are simulated.
512 devices in a mesh: grp: 2 (over y), kv: 16 (over z), tp: 16 (over x, core).
Axes of the slice: x: 8, y: 2, z: 16, core: 2. Of those that a mesh axis runs over, the one named last changes fastest.
The devices are a block of a 8x16x16 slice.
Arguments:
- tokens: bfloat16 [256, 4096], P('grp', 'kv'), parts along dimension 0, may hold values from -36 to 36
- span_lengths: int32 [256], P(('grp', 'kv')), parts along dimension 0, may hold values from 1 to 256, 13107 in all
- block_state: float32 [256, 64, 32, 64], P(('grp', 'kv'), 'tp'), parts along dimension 0, may hold values from -96 to 96
- key_cache: bfloat16 [256, 2048, 256], P(('grp', 'kv'), 'tp'), parts along dimension 0, may hold values from -6 to 6
- value_cache: bfloat16 [256, 4096, 256], P(('grp', 'kv'), 'tp'), parts along dimension 0, may hold values from -6 to 6
- decay_cache: float32 [256, 2048, 256], P(('grp', 'kv'), 'tp'), parts along dimension 0, may hold values from -34 to 0, as said below
- attn_gain: float32 [4096], P('kv'), may hold values from 0.1 to 1.9
- query_weight: bfloat16 [4096, 2048], P('kv', 'tp'), may hold values from -0.09375 to 0.09375
- key_weight: bfloat16 [4096, 2048], P('kv', 'tp'), may hold values from -0.09375 to 0.09375
- value_weight: bfloat16 [4096, 4096], P('kv', 'tp'), may hold values from -0.09375 to 0.09375
- gate_weight: bfloat16 [4096, 4096], P('kv', 'tp'), may hold values from -0.09375 to 0.09375
- decay_matrix: bfloat16 [4096, 2048], P('kv', 'tp'), may hold values from -0.09375 to 0.09375
- decay_offset_bias: float32 [2048], P('tp'), may hold values from -1.4 to 6
- head_gain: float32 [64], replicated, may hold values from 0.1 to 1.9
- out_weight: bfloat16 [4096, 4096], P('tp', 'kv'), may hold values from -0.09375 to 0.09375
- mixer_gain: float32 [4096], P('kv'), may hold values from 0.1 to 1.9
- up_weight: bfloat16 [4096, 16384], P('kv', 'tp'), may hold values from -0.09375 to 0.09375
- down_weight: bfloat16 [16384, 4096], P('tp', 'kv'), may hold values from -0.046875 to 0.046875
Outputs:
- layer_out: bfloat16 [256, 4096], P('grp', 'kv'), parts along dimension 0
There are 2 independent parts, one for each index of `grp`. A program takes and returns all parts, laid end to end along the dimension named above; an argument that names none is the same for every part. Nothing has to cross between parts.
Inputs may be any that keep to these rules, and one draw needn't show every extreme that they name: Cached positions at index span_lengths - 1 and beyond are unused. `decay_cache`: Non-increasing along positions.
All inputs are finite; a program needn't handle non-finite values. No bound on the sum of `span_lengths` on one device may be relied on, other than what follows from the above.
Results may differ from a plain program's by a relative error of at most 0.005.
The roundings to bfloat16 on the way count: a program that leaves them out, or rounds other values in their place, can miss the bound.
Values may be sent and summed in bfloat16 or wider, within the bound.
No kernel may reach another device: no remote copies, remote signals or barrier semaphores. Data moves between devices by JAX's collectives and lax.ppermute only.
A program may use at most 64 MiB of HBM per device.

v0:
```python
import math

import jax
import jax.numpy as jnp
from jax import lax
from jax.sharding import PartitionSpec as P

D = 4096
KEY_WIDTH = 32
DV = 64


NORM_EPS = 1e-06
DECAY_SOFTNESS = 16.0


def cut_along(value, dim, peers):
    before, after = (value.shape[:dim], value.shape[dim + 1 :])
    return jnp.moveaxis(value.reshape(*before, peers, -1, *after), dim, 0)


def sum_at_owner(value, axis, dim):
    pieces = cut_along(value, dim, lax.axis_size(axis))
    arrived = lax.all_to_all(pieces, axis, split_axis=0, concat_axis=0, tiled=True)
    return arrived.sum(axis=0)


def side_by_side(arrays, axis, dim, along):
    widths = [math.prod(a.shape[along:]) for a in arrays]
    both = jnp.concatenate(
        [a.reshape(*a.shape[:along], w) for a, w in zip(arrays, widths)], axis=along
    )
    filled = sum_at_owner(both, axis, dim)
    pieces = jnp.split(filled, [sum(widths[:k]) for k in range(1, len(widths))], axis=along)
    return tuple(
        (b.reshape(*filled.shape[:along], *a.shape[along:]) for a, b in zip(arrays, pieces))
    )


def from_everyone(value, axis):
    peers = lax.axis_size(axis)
    return lax.all_to_all(
        jnp.broadcast_to(value[None], (peers, *value.shape)), axis, 0, 0, tiled=True
    )


def laid_out(pieces, dim):
    pieces = jnp.moveaxis(pieces, 0, dim)
    dims = pieces.shape
    return pieces.reshape(*dims[:dim], dims[dim] * dims[dim + 1], *dims[dim + 2 :])


def collect(value, axis, dim):
    pieces = from_everyone(value, axis)
    return laid_out(pieces, dim)


def rows_for(lines, peers):
    spare = -len(lines) % peers
    return jnp.pad(lines, [(0, spare)] + [(0, 0)] * (lines.ndim - 1))


def nested_sum(value, axes):
    lines = value.reshape(-1, value.shape[-1])
    padded = rows_for(lines, lax.axis_size(axes))
    whole = collect(sum_at_owner(padded, axes, 0), axes, 0)
    return lax.slice_in_dim(whole, 0, len(lines)).reshape(value.shape)


def shards(
    tokens,
    span_lengths,
    block_state,
    key_cache,
    value_cache,
    decay_cache,
    attn_gain,
    query_weight,
    key_weight,
    value_weight,
    gate_weight,
    decay_matrix,
    decay_offset_bias,
    head_gain,
    out_weight,
    mixer_gain,
    up_weight,
    down_weight,
):
    seq_count = block_state.shape[0]
    head_count = block_state.shape[1]
    span_size = key_cache.shape[2]
    whole_rows = tokens.astype(jnp.float32)
    square_sum = jnp.sum(whole_rows * whole_rows, axis=1)
    scaled = (whole_rows * attn_gain).astype(jnp.bfloat16)
    query_part = jnp.dot(scaled, query_weight, preferred_element_type=jnp.float32)
    key_part = jnp.dot(scaled, key_weight, preferred_element_type=jnp.float32)
    value_part = jnp.dot(scaled, value_weight, preferred_element_type=jnp.float32)
    gate_part = jnp.dot(scaled, gate_weight, preferred_element_type=jnp.float32)
    decay_part = jnp.dot(scaled, decay_matrix, preferred_element_type=jnp.float32)
    query_sum, key_sum, value_sum, gate_sum, decay_running_sum, own_square = side_by_side(
        (query_part, key_part, value_part, gate_part, decay_part, square_sum), "kv", 0, 1
    )
    scale_per_row = lax.rsqrt(own_square / D + NORM_EPS)[:, None]
    query = (query_sum * scale_per_row * KEY_WIDTH ** (-0.5)).reshape(
        seq_count, head_count, KEY_WIDTH
    )
    key_new = (key_sum * scale_per_row).reshape(seq_count, head_count, KEY_WIDTH)
    value_new = (value_sum * scale_per_row).reshape(seq_count, head_count, DV)
    gate = gate_sum * scale_per_row
    logarithm_decay = (
        jax.nn.log_sigmoid(decay_running_sum * scale_per_row + decay_offset_bias) / DECAY_SOFTNESS
    )
    token_place = lax.broadcasted_iota(jnp.int32, (1, 1, span_size), 2)
    lengths_now = span_lengths[:, None, None]
    previous = jnp.sum(jnp.where(token_place == lengths_now - 2, decay_cache, 0.0), axis=-1)
    now_decay = (previous + logarithm_decay).reshape(seq_count, head_count, KEY_WIDTH)
    decays_span = decay_cache.reshape(seq_count, head_count, KEY_WIDTH, span_size)
    in_use = (token_place < lengths_now - 1)[:, :, None, :]
    factor = jnp.where(in_use, jnp.exp(now_decay[..., None] - decays_span), 0.0)
    keys_span = key_cache.reshape(seq_count, head_count, KEY_WIDTH, span_size)
    scores = jnp.sum(query[..., None] * keys_span.astype(jnp.float32) * factor, axis=2)
    scores_low = scores.astype(jnp.bfloat16)
    values_span = value_cache.reshape(seq_count, head_count, DV, span_size)
    history = jnp.einsum(
        "nhs,nhvs->nhv", scores_low, values_span, preferred_element_type=jnp.float32
    )
    carried = jnp.einsum(
        "nhc,nhcv->nhv", query * jnp.exp(now_decay), block_state, precision=lax.Precision.HIGHEST
    )
    own_term = jnp.sum(query * key_new, axis=-1, keepdims=True) * value_new
    raw = carried + history + own_term
    normed = raw * lax.rsqrt(jnp.mean(raw * raw, axis=-1, keepdims=True) + NORM_EPS) * head_gain
    mixed = (normed.reshape(seq_count, head_count * DV) * jax.nn.silu(gate)).astype(jnp.bfloat16)
    attn_terms = jnp.dot(collect(mixed, "kv", 0), out_weight, preferred_element_type=jnp.float32)
    attn_out = nested_sum(attn_terms, "tp")
    resid = (whole_rows + attn_out).astype(jnp.bfloat16)
    resid_rows = resid.astype(jnp.float32)
    mixer_square = jnp.sum(resid_rows * resid_rows, axis=1)
    mixer_scaled = (resid_rows * mixer_gain).astype(jnp.bfloat16)
    up_part = jnp.dot(mixer_scaled, up_weight, preferred_element_type=jnp.float32)
    up_share, square_share = side_by_side((up_part, mixer_square), "kv", 0, 1)
    hidden_share = jnp.square(
        jax.nn.relu(up_share * lax.rsqrt(square_share / D + NORM_EPS)[:, None])
    )
    hidden_share = hidden_share.astype(jnp.bfloat16)
    down_terms = jnp.dot(
        collect(hidden_share, "kv", 0), down_weight, preferred_element_type=jnp.float32
    )
    mixer_out = nested_sum(down_terms, "tp")
    return (resid_rows + mixer_out).astype(jnp.bfloat16)


def solution(mesh):
    placed = (
        P("grp", "kv"),
        P(("grp", "kv")),
        P(("grp", "kv"), "tp", None, None),
        P(("grp", "kv"), "tp", None),
        P(("grp", "kv"), "tp", None),
        P(("grp", "kv"), "tp", None),
        P("kv"),
        P("kv", "tp"),
        P("kv", "tp"),
        P("kv", "tp"),
        P("kv", "tp"),
        P("kv", "tp"),
        P("tp"),
        P(),
        P("tp", "kv"),
        P("kv"),
        P("kv", "tp"),
        P("tp", "kv"),
    )
    return jax.shard_map(
        shards, mesh=mesh, in_specs=placed, out_specs=P("grp", "kv"), check_vma=False
    )
```

profile of v0, /device:TPU:65, one launch (start us, length us, event | category | flops | bytes accessed | tf_op | source)
XLA Modules:
  0.0 217.7 jit_solution(4362667146889615148)
XLA Ops:
  0.0 1.0 fusion.10
  1.1 0.2 concatenate.34
  1.3 0.5 copy-done.13
  1.7 0.8 fusion.4
  2.6 0.8 fusion.3
  3.5 0.8 fusion.1
  4.3 0.8 fusion
  5.2 0.8 fusion.2
  6.0 0.6 constant_dynamic-update-slice_fusion
  6.6 44.3 %all-to-all-start = ((f32[16,8,897]{2,1,0:T(8,128)}), f32[16,8,897]{2,1,0:T(8,128)S(1)}, u32[]{:S(2)}, u32[]{:S(2)}) async-start(f32[16,8,897]{2,1,0:T(8,128)} %constant_dynamic-update-slice_fusion), calls=%async_computation | async-start | bytes 1048576 | tf_op jit(solution)/shard_map/all_to_all | solution.py:24
  51.0 0.2 select_reduce_fusion
  51.3 22.4 %all-to-all-done = f32[16,8,897]{2,1,0:T(8,128)S(1)} async-done(((f32[16,8,897]{2,1,0:T(8,128)}), f32[16,8,897]{2,1,0:T(8,128)S(1)}, u32[]{:S(2)}, u32[]{:S(2)}) %all-to-all-start) | async-done | bytes 459296 | tf_op jit(solution)/shard_map/all_to_all | solution.py:24
  74.0 0.6 copy-done.16
  75.0 0.5 fusion.6
  75.5 0.4 fusion.22
  75.9 0.7 copy-done.6
  76.6 0.5 fusion.42
  77.1 0.2 multiply_reduce_fusion
  77.3 0.7 copy-done.15
  78.2 23.7 %all_to_all.40 = bf16[16,8,256]{2,1,0:T(8,128)(2,1)S(1)} all-to-all(bf16[16,8,256]{2,1,0:T(8,128)(2,1)S(1)} %broadcast_in_dim.36), channel_id=1, replica_groups=mesh['grp'=2,'kv'=16,'tp'=16] {'kv'}, dimensions={0} | all-to-all | bytes 131072 | tf_op jit(solution)/shard_map/all_to_all | solution.py:42
  101.9 0.2 fusion.15
  102.1 18.5 %all_to_all.41 = f32[16,8,256]{2,1,0:T(8,128)S(1)} all-to-all(f32[16,8,256]{2,1,0:T(8,128)S(1)} %fusion.15), channel_id=1, replica_groups=mesh['grp'=2,'kv'=16,'tp'=16] {'tp'}, dimensions={0} | all-to-all | bytes 262144 | tf_op jit(solution)/shard_map/all_to_all | solution.py:24
  120.6 11.6 %all_to_all.42 = f32[16,8,256]{2,1,0:T(8,128)S(1)} all-to-all(f32[16,8,256]{2,1,0:T(8,128)S(1)} %broadcast_in_dim.37), channel_id=1, replica_groups=mesh['grp'=2,'kv'=16,'tp'=16] {'tp'}, dimensions={0} | all-to-all | bytes 262144 | tf_op jit(solution)/shard_map/all_to_all | solution.py:42
  132.3 0.2 concatenate.35
  132.5 0.7 copy-done.14
  133.2 0.2 convolution_bitcast_fusion
  133.5 36.7 %all_to_all.43 = f32[16,8,1025]{2,1,0:T(8,128)S(1)} all-to-all(f32[16,8,1025]{2,1,0:T(8,128)S(1)} %pad_maximum_fusion), channel_id=1, replica_groups=mesh['grp'=2,'kv'=16,'tp'=16] {'kv'}, dimensions={0} | all-to-all | bytes 1049600 | tf_op jit(solution)/shard_map/all_to_all | solution.py:24
  170.4 17.8 %all_to_all.44 = bf16[16,8,1024]{2,1,0:T(8,128)(2,1)S(1)} all-to-all(bf16[16,8,1024]{2,1,0:T(8,128)(2,1)S(1)} %broadcast_in_dim.38), channel_id=1, replica_groups=mesh['grp'=2,'kv'=16,'tp'=16] {'kv'}, dimensions={0} | all-to-all | bytes 524288 | tf_op jit(solution)/shard_map/all_to_all | solution.py:42
  188.2 0.2 fusion.7
  188.5 17.2 %all_to_all.45 = f32[16,8,256]{2,1,0:T(8,128)S(1)} all-to-all(f32[16,8,256]{2,1,0:T(8,128)S(1)} %fusion.7), channel_id=1, replica_groups=mesh['grp'=2,'kv'=16,'tp'=16] {'tp'}, dimensions={0} | all-to-all | bytes 262144 | tf_op jit(solution)/shard_map/all_to_all | solution.py:24
  205.7 11.3 %all_to_all.46 = f32[16,8,256]{2,1,0:T(8,128)S(1)} all-to-all(f32[16,8,256]{2,1,0:T(8,128)S(1)} %broadcast_in_dim.39), channel_id=1, replica_groups=mesh['grp'=2,'kv'=16,'tp'=16] {'tp'}, dimensions={0} | all-to-all | bytes 262144 | tf_op jit(solution)/shard_map/all_to_all | solution.py:42
  217.1 0.6 fusion.14
  (58 shorter events, 1.8 us)
Async XLA Ops:
  0.0 75.5 %copy-start = (bf16[8,256,256]{2,1,0:T(8,128)(2,1)S(1)}, bf16[8,256,256]{2,1,0:T(8,128)(2,1)}, u32[]{:S(2)}) copy-start(bf16[8,256,256]{2,1,0:T(8,128)(2,1)} %param.22) | copy-start | bytes 3145732
  0.0 1.3 copy-start.2
  0.0 1.3 copy-start.10
  1.1 0.7 copy-start.13
  1.7 0.8 copy-start.11
  2.6 0.9 copy-start.7
  2.6 1.8 copy-start.8
  2.6 2.6 %copy-start.12 = (bf16[256,128]{1,0:T(8,128)(2,1)S(1)}, bf16[256,128]{1,0:T(8,128)(2,1)}, u32[]{:S(2)}) copy-start(bf16[256,128]{1,0:T(8,128)(2,1)} %param.29) | copy-start | bytes 196612
  3.5 47.6 %copy-start.1 = (f32[8,128,256]{2,1,0:T(8,128)S(1)}, f32[8,128,256]{2,1,0:T(8,128)}, u32[]{:S(2)}) copy-start(f32[8,128,256]{2,1,0:T(8,128)} %param.23) | copy-start | bytes 3145732
  6.6 44.4 %copy-start.17 = (s32[8]{0:T(128)S(1)}, s32[8]{0:T(128)}, u32[]{:S(2)}) copy-start(s32[8]{0:T(128)} %param.19) | copy-start | bytes 100
  6.6 67.1 %all-to-all-start = ((f32[16,8,897]{2,1,0:T(8,128)}), f32[16,8,897]{2,1,0:T(8,128)S(1)}, u32[]{:S(2)}, u32[]{:S(2)}) async-start(f32[16,8,897]{2,1,0:T(8,128)} %constant_dynamic-update-slice_fusion), calls=%async_computation | async-start | bytes 1048576 | tf_op jit(solution)/shard_map/all_to_all | solution.py:24
  51.3 23.8 %copy-start.5 = (bf16[8,128,256]{2,1,0:T(8,128)(2,1)S(1)}, bf16[8,128,256]{2,1,0:T(8,128)(2,1)}, u32[]{:S(2)}) copy-start(bf16[8,128,256]{2,1,0:T(8,128)(2,1)} %param.21) | copy-start | bytes 1572868
  73.9 0.7 copy-start.16
  75.5 1.0 copy-start.6
  77.3 0.7 copy-start.15
  78.0 23.9 %copy-start.9 = (bf16[256,256]{1,0:T(8,128)(2,1)S(1)}, bf16[256,256]{1,0:T(8,128)(2,1)}, u32[]{:S(2)}) copy-start(bf16[256,256]{1,0:T(8,128)(2,1)} %param.32) | copy-start | bytes 393220
  102.1 30.4 %copy-start.3 = (bf16[256,1024]{1,0:T(8,128)(2,1)S(1)}, bf16[256,1024]{1,0:T(8,128)(2,1)}, u32[]{:S(2)}) copy-start(bf16[256,1024]{1,0:T(8,128)(2,1)} %param.34) | copy-start | bytes 1572868
  132.5 0.7 copy-start.14
  170.2 18.1 %copy-start.4 = (bf16[1024,256]{1,0:T(8,128)(2,1)S(1)}, bf16[1024,256]{1,0:T(8,128)(2,1)}, u32[]{:S(2)}) copy-start(bf16[1024,256]{1,0:T(8,128)(2,1)} %param.35) | copy-start | bytes 1572868
where the time goes:
time: 218 us
  blocking collectives  137 us (63%)
  starting transfers between devices  44.3 us (20%)
  waiting for transfers between devices  22.4 us (10%)
  matrix products  5.58 us (3%)
  local copies, waits for them, and re-layouts  4.71 us (2%)
  other arithmetic  3.65 us (2%)
    all_to_all x3, blocking collectives, sum_at_owner(): lax.all_to_all(pieces, axis, split_axis=0, concat_axis=0, tiled=True)  72.4 us
    all_to_all x4, blocking collectives, from_everyone(): lax.all_to_all(jnp.broadcast_to(value[None], (peers, *value.shape)), axis...  64.4 us
    all_to_all x1, starting transfers between devices, sum_at_owner(): lax.all_to_all(pieces, axis, split_axis=0, concat_axis=0, tiled=True)  44.3 us
    all_to_all x1, waiting for transfers between devices, sum_at_owner(): lax.all_to_all(pieces, axis, split_axis=0, concat_axis=0, tiled=True)  22.4 us
  transfers between devices with their start and end apart: 1, of which 1 were waited for; matrix products, arithmetic and copies ran while one was open for 0% of the time, Pallas kernels for 0%

commit v1 on v0

v1 whole, which is shorter than its diff:
```python
import jax
import jax.numpy as jnp
from jax import lax
from jax.sharding import Mesh, PartitionSpec as P

D = 4096
KEY_WIDTH = 32
DV = 64
LANES = 128
CORES = 2

NORM_EPS = 1e-06
DECAY_SOFTNESS = 16.0


def exchange(pieces, axes):
    return lax.all_to_all(pieces, axes, 0, 0, tiled=True)


def to_everyone(value, axes):
    peers = lax.axis_size(axes)
    return exchange(jnp.broadcast_to(value[None], (peers, *value.shape)), axes)


def square_lanes(square):
    high = lax.reduce_precision(square, 8, 7)
    low = (square - high).astype(jnp.bfloat16)
    both = jnp.concatenate([high.astype(jnp.bfloat16), low], axis=1)
    return jnp.pad(both, [(0, 0), (0, LANES - both.shape[1])])


def dot(a, b):
    return jnp.dot(a, b, preferred_element_type=jnp.float32)


def shards(
    tokens,
    span_lengths,
    block_state,
    key_cache,
    value_cache,
    decay_cache,
    attn_gain,
    query_weight,
    key_weight,
    value_weight,
    gate_weight,
    decay_matrix,
    decay_offset_bias,
    head_gain,
    out_weight,
    mixer_gain,
    up_weight,
    down_weight,
):
    f32, bf16 = jnp.float32, jnp.bfloat16
    seq_count, head_count = block_state.shape[:2]
    span_size = key_cache.shape[2]
    peers = lax.axis_size("kv")
    core = lax.axis_index("core")
    half = seq_count // CORES
    rows_half = peers * half
    keys, values = head_count * KEY_WIDTH, head_count * DV

    whole_rows = tokens.astype(f32)
    square_sum = jnp.sum(whole_rows * whole_rows, axis=1, keepdims=True)
    scaled = (whole_rows * attn_gain).astype(bf16)
    parts = [
        dot(scaled, w).astype(bf16)
        for w in (query_weight, key_weight, decay_matrix, value_weight, gate_weight)
    ]
    sent = jnp.concatenate([*parts, square_lanes(square_sum)], axis=1)
    arrived = exchange(sent.reshape(peers, seq_count, -1), "kv")

    swap = [(c, CORES - 1 - c) for c in range(CORES)]
    out_other = lax.ppermute(out_weight, "core", swap)
    up_other = lax.ppermute(up_weight, "core", swap)
    down_other = lax.ppermute(down_weight, "core", swap)
    out_first = jnp.where(core == 0, out_weight, out_other)
    out_second = jnp.where(core == 0, out_other, out_weight)
    own_tokens = lax.dynamic_index_in_dim(
        tokens.reshape(peers, CORES, half, -1), core, 1, keepdims=False
    ).reshape(rows_half, -1)

    total = jnp.sum(arrived.astype(f32), axis=0)
    query_sum, key_sum, decay_sum, value_sum, gate_sum, squares = jnp.split(
        total, [keys, 2 * keys, 3 * keys, 3 * keys + values, 3 * keys + 2 * values], axis=1
    )
    scale_per_row = lax.rsqrt((squares[:, :1] + squares[:, 1:2]) / D + NORM_EPS)
    query = (query_sum * scale_per_row * KEY_WIDTH ** (-0.5)).reshape(
        seq_count, head_count, KEY_WIDTH
    )
    key_new = (key_sum * scale_per_row).reshape(seq_count, head_count, KEY_WIDTH)
    value_new = (value_sum * scale_per_row).reshape(seq_count, head_count, DV)
    gate = gate_sum * scale_per_row
    logarithm_decay = (
        jax.nn.log_sigmoid(decay_sum * scale_per_row + decay_offset_bias) / DECAY_SOFTNESS
    )
    token_place = lax.broadcasted_iota(jnp.int32, (1, 1, span_size), 2)
    lengths_now = span_lengths[:, None, None]
    previous = jnp.sum(jnp.where(token_place == lengths_now - 2, decay_cache, 0.0), axis=-1)
    now_decay = (previous + logarithm_decay).reshape(seq_count, head_count, KEY_WIDTH)
    decays_span = decay_cache.reshape(seq_count, head_count, KEY_WIDTH, span_size)
    in_use = (token_place < lengths_now - 1)[:, :, None, :]
    factor = jnp.where(in_use, jnp.exp(now_decay[..., None] - decays_span), 0.0)
    keys_span = key_cache.reshape(seq_count, head_count, KEY_WIDTH, span_size)
    scores = jnp.sum(query[..., None] * keys_span.astype(f32) * factor, axis=2)
    scores_low = scores.astype(bf16)
    values_span = value_cache.reshape(seq_count, head_count, DV, span_size)
    history = jnp.einsum("nhs,nhvs->nhv", scores_low, values_span, preferred_element_type=f32)
    carried = jnp.einsum(
        "nhc,nhcv->nhv", query * jnp.exp(now_decay), block_state, precision=lax.Precision.HIGHEST
    )
    own_term = jnp.sum(query * key_new, axis=-1, keepdims=True) * value_new
    raw = carried + history + own_term
    normed = raw * lax.rsqrt(jnp.mean(raw * raw, axis=-1, keepdims=True) + NORM_EPS) * head_gain
    mixed = (normed.reshape(seq_count, values) * jax.nn.silu(gate)).astype(bf16)

    spread = jnp.broadcast_to(
        mixed.reshape(1, CORES, half, values), (peers, CORES, half, values)
    ).reshape(peers * CORES, half, values)
    heads = exchange(spread, ("kv", "core")).reshape(peers, CORES, half, values)
    attn_terms = dot(heads[:, 0].reshape(rows_half, values), out_first) + dot(
        heads[:, 1].reshape(rows_half, values), out_second
    )
    attn_out = jnp.sum(to_everyone(attn_terms.astype(bf16), "x").astype(f32), axis=0)
    resid = (own_tokens.astype(f32) + attn_out).astype(bf16)
    resid_rows = resid.astype(f32)
    mixer_square = jnp.sum(resid_rows * resid_rows, axis=1, keepdims=True)
    mixer_scaled = (resid_rows * mixer_gain).astype(bf16)
    up_sent = jnp.concatenate(
        [
            dot(mixer_scaled, up_weight).astype(bf16),
            dot(mixer_scaled, up_other).astype(bf16),
            square_lanes(mixer_square),
        ],
        axis=1,
    )
    up_total = jnp.sum(exchange(up_sent.reshape(peers, half, -1), "kv").astype(f32), axis=0)
    hidden_count = up_weight.shape[1] * CORES
    before, squares = up_total[:, :hidden_count], up_total[:, hidden_count:]
    mixer_scale = lax.rsqrt((squares[:, :1] + squares[:, 1:2]) / D + NORM_EPS)
    hidden = jnp.square(jax.nn.relu(before * mixer_scale)).astype(bf16)
    every = to_everyone(hidden, "kv").reshape(rows_half, hidden_count)
    own_count = up_weight.shape[1]
    down_terms = dot(every[:, :own_count], down_weight) + dot(every[:, own_count:], down_other)
    mixer_out = jnp.sum(to_everyone(down_terms.astype(bf16), "x").astype(f32), axis=0)
    own_out = (resid_rows + mixer_out).astype(bf16)
    both = to_everyone(own_out, "core").reshape(CORES, peers, half, -1)
    return jnp.swapaxes(both, 0, 1).reshape(peers * seq_count, -1)


def solution(mesh):
    sizes = dict(mesh.shape)
    fine = Mesh(
        mesh.devices.reshape(sizes["grp"], sizes["kv"], sizes["tp"] // CORES, CORES),
        ("grp", "kv", "x", "core"),
    )
    tp = ("x", "core")
    placed = (
        P("grp", "kv"),
        P(("grp", "kv")),
        P(("grp", "kv"), tp, None, None),
        P(("grp", "kv"), tp, None),
        P(("grp", "kv"), tp, None),
        P(("grp", "kv"), tp, None),
        P("kv"),
        P("kv", tp),
        P("kv", tp),
        P("kv", tp),
        P("kv", tp),
        P("kv", tp),
        P(tp),
        P(),
        P(tp, "kv"),
        P("kv"),
        P("kv", tp),
        P(tp, "kv"),
    )
    return jax.shard_map(
        shards, mesh=fine, in_specs=placed, out_specs=P("grp", "kv"), check_vma=False
    )
```

time: 218 us -> 186 us (0.85)
  blocking collectives: 137 us -> 41 us
  starting transfers between devices: 44.3 us -> 83.8 us
  waiting for transfers between devices: 22.4 us -> 39.3 us
  local copies, waits for them, and re-layouts: 4.71 us -> 9.41 us
  matrix products: 5.58 us -> 7.84 us
    all_to_all x7 -> x3, blocking collectives: 137 us -> 41 us  [exchange(): return lax.all_to_all(pieces, axes, 0, 0, tiled=True)]
    all_to_all x1 -> x4, starting transfers between devices: 44.3 us -> 74.4 us  [exchange(): return lax.all_to_all(pieces, axes, 0, 0, tiled=True)]
    all_to_all x1 -> x4, waiting for transfers between devices: 22.4 us -> 39.3 us  [exchange(): return lax.all_to_all(pieces, axes, 0, 0, tiled=True)]
    ppermute x0 -> x3, starting transfers between devices: none -> 9.42 us  [the longest x1 3.83 us: shards(): up_other = lax.ppermute(up_weight, 'core', swap)]
    dot_general x8 -> x11, matrix products: 4.69 us -> 6.94 us  [dot(): return jnp.dot(a, b, preferred_element_type=jnp.float32)]
    unnamed x36 -> x31, local copies, waits for them, and re-layouts: 3.23 us -> 4.48 us
  transfers between devices with their start and end apart: 1 -> 7, of which waited for: 1 -> 4; matrix products, arithmetic and copies ran while one was open for 0% -> 1% of each run, Pallas kernels for 0% -> 0%
where the time goes in v1:
time: 186 us; the launch traced here: 185 us
  starting transfers between devices  83.8 us (45%)
  blocking collectives  41 us (22%)
  waiting for transfers between devices  39.3 us (21%)
  local copies, waits for them, and re-layouts  9.41 us (5%)
  matrix products  7.84 us (4%)
  other arithmetic  3.4 us (2%)
    all_to_all x4, starting transfers between devices, exchange(): return lax.all_to_all(pieces, axes, 0, 0, tiled=True)  74.4 us
    all_to_all x3, blocking collectives, exchange(): return lax.all_to_all(pieces, axes, 0, 0, tiled=True)  41 us
    all_to_all x4, waiting for transfers between devices, exchange(): return lax.all_to_all(pieces, axes, 0, 0, tiled=True)  39.3 us
    dot_general x11, matrix products, dot(): return jnp.dot(a, b, preferred_element_type=jnp.float32)  6.94 us
    unnamed x31, local copies, waits for them, and re-layouts  4.48 us
    ppermute x1, starting transfers between devices, shards(): up_other = lax.ppermute(up_weight, 'core', swap)  3.83 us
  transfers between devices with their start and end apart: 7, of which 4 were waited for; matrix products, arithmetic and copies ran while one was open for 1% of the time, Pallas kernels for 0%

profile of v1, /device:TPU:65, one launch (start us, length us, event | category | flops | bytes accessed | tf_op | source)
XLA Modules:
  0.0 185.2 jit_solution(1363420375216686671)
XLA Ops:
  0.0 1.1 fusion.9
  1.3 1.1 convolution_convert_fusion.6
  2.5 1.1 convolution_convert_fusion.5
  3.7 1.1 convolution_convert_fusion.4
  4.9 0.6 constant_dynamic-update-slice_fusion.2
  5.5 0.6 constant_dynamic-update-slice_fusion.1
  6.1 0.6 constant_dynamic-update-slice_fusion
  6.8 1.8 fusion.1
  8.5 0.8 fusion
  9.3 0.6 pad_dynamic-update-slice_fusion
  10.0 44.4 %all-to-all-start = ((bf16[16,8,1024]{2,1,0:T(8,128)(2,1)}), bf16[16,8,1024]{2,1,0:T(8,128)(2,1)S(1)}, u32[]{:S(2)}, u32[]{:S(2)}) async-start(bf16[16,8,1024]{2,1,0:T(8,128)(2,1)} %bitcast.1), calls=%async_computation | async-start | bytes 524288 | tf_op jit(solution)/shard_map/all_to_all | solution.py:17
  54.7 13.2 %all-to-all-done = bf16[16,8,1024]{2,1,0:T(8,128)(2,1)S(1)} async-done(((bf16[16,8,1024]{2,1,0:T(8,128)(2,1)}), bf16[16,8,1024]{2,1,0:T(8,128)(2,1)S(1)}, u32[]{:S(2)}, u32[]{:S(2)}) %all-to-all-start) | async-done | bytes 262176 | tf_op jit(solution)/shard_map/all_to_all | solution.py:17
  68.3 0.6 copy-done.12
  70.2 0.7 copy-done.4
  71.5 0.7 copy-done.11
  72.4 0.7 broadcast_in_dim.41
  73.1 11.6 %all-to-all-start.1 = ((bf16[32,4,256]{2,1,0:T(4,128)(2,1)}), bf16[32,4,256]{2,1,0:T(4,128)(2,1)S(1)}, u32[]{:S(2)}, u32[]{:S(2)}) async-start(bf16[32,4,256]{2,1,0:T(4,128)(2,1)} %bitcast.12), calls=%async_computation.1 | async-start | bytes 131072 | tf_op jit(solution)/shard_map/all_to_all | solution.py:17
  84.7 2.6 %collective-permute-start = (bf16[256,256]{1,0:T(8,128)(2,1)S(1)}, bf16[256,256]{1,0:T(8,128)(2,1)S(1)}, u32[]{:S(2)}, u32[]{:S(2)}) collective-permute-start(bf16[256,256]{1,0:T(8,128)(2,1)S(1)} %copy-done.7), channel_id=1, source_target_pairs={{0,1},{1,0},{2,3},{3,2},{4,5},{5,4},{6,7},{7,6},{8,9},{9,8},{10,11... | collective-permute-start | bytes 393224 | tf_op jit(solution)/shard_map/ppermute | solution.py:76
  87.4 10.1 %all-to-all-done.1 = bf16[32,4,256]{2,1,0:T(4,128)(2,1)S(1)} async-done(((bf16[32,4,256]{2,1,0:T(4,128)(2,1)}), bf16[32,4,256]{2,1,0:T(4,128)(2,1)S(1)}, u32[]{:S(2)}, u32[]{:S(2)}) %all-to-all-start.1) | async-done | bytes 65568 | tf_op jit(solution)/shard_map/all_to_all | solution.py:17
  97.9 0.7 broadcast_in_dim.42
  98.6 7.0 %all-to-all-start.2 = ((bf16[8,64,256]{2,1,0:T(8,128)(2,1)}), bf16[8,64,256]{2,1,0:T(8,128)(2,1)S(1)}, u32[]{:S(2)}, u32[]{:S(2)}) async-start(bf16[8,64,256]{2,1,0:T(8,128)(2,1)} %broadcast_in_dim.42), calls=%async_computation.2 | async-start | bytes 524288 | tf_op jit(solution)/shard_map/all_to_all | solution.py:17
  105.7 3.8 %collective-permute-start.1 = (bf16[256,1024]{1,0:T(8,128)(2,1)S(1)}, bf16[256,1024]{1,0:T(8,128)(2,1)S(1)}, u32[]{:S(2)}, u32[]{:S(2)}) collective-permute-start(bf16[256,1024]{1,0:T(8,128)(2,1)S(1)} %copy-done.5), channel_id=1, source_target_pairs={{0,1},{1,0},{2,3},{3,2},{4,5},{5,4},{6,7},{7,6},{8,9},{9,8},{10,11... | collective-permute-start | bytes 1572872 | tf_op jit(solution)/shard_map/ppermute | solution.py:77
  109.6 5.4 %all-to-all-done.2 = bf16[8,64,256]{2,1,0:T(8,128)(2,1)S(1)} async-done(((bf16[8,64,256]{2,1,0:T(8,128)(2,1)}), bf16[8,64,256]{2,1,0:T(8,128)(2,1)S(1)}, u32[]{:S(2)}, u32[]{:S(2)}) %all-to-all-start.2) | async-done | bytes 262176 | tf_op jit(solution)/shard_map/all_to_all | solution.py:17
  115.4 0.7 copy-done.10
  116.6 18.9 %all_to_all.35 = bf16[16,4,2176]{2,1,0:T(4,128)(2,1)S(1)} all-to-all(bf16[16,4,2176]{2,1,0:T(4,128)(2,1)S(1)} %reshape.201), channel_id=1, replica_groups=mesh['grp'=2,'kv'=16,'x'=8,'core'=2] {'kv'}, dimensions={0} | all-to-all | bytes 557056 | tf_op jit(solution)/shard_map/all_to_all | solution.py:17
  135.9 0.8 broadcast_in_dim.43
  136.7 11.4 %all-to-all-start.4 = ((bf16[16,4,2048]{2,1,0:T(4,128)(2,1)}), bf16[16,4,2048]{2,1,0:T(4,128)(2,1)S(1)}, u32[]{:S(2)}, u32[]{:S(2)}) async-start(bf16[16,4,2048]{2,1,0:T(4,128)(2,1)} %broadcast_in_dim.43), calls=%async_computation.4 | async-start | bytes 524288 | tf_op jit(solution)/shard_map/all_to_all | solution.py:17
  148.1 2.9 %collective-permute-start.2 = (bf16[1024,256]{1,0:T(8,128)(2,1)S(1)}, bf16[1024,256]{1,0:T(8,128)(2,1)S(1)}, u32[]{:S(2)}, u32[]{:S(2)}) collective-permute-start(bf16[1024,256]{1,0:T(8,128)(2,1)S(1)} %copy-done.6), channel_id=1, source_target_pairs={{0,1},{1,0},{2,3},{3,2},{4,5},{5,4},{6,7},{7,6},{8,9},{9,8},{10,11... | collective-permute-start | bytes 1572872 | tf_op jit(solution)/shard_map/ppermute | solution.py:78
  151.1 10.6 %all-to-all-done.4 = bf16[16,4,2048]{2,1,0:T(4,128)(2,1)S(1)} async-done(((bf16[16,4,2048]{2,1,0:T(4,128)(2,1)}), bf16[16,4,2048]{2,1,0:T(4,128)(2,1)S(1)}, u32[]{:S(2)}, u32[]{:S(2)}) %all-to-all-start.4) | async-done | bytes 262176 | tf_op jit(solution)/shard_map/all_to_all | solution.py:17
  162.2 11.8 %all_to_all.36 = bf16[8,64,256]{2,1,0:T(8,128)(2,1)S(1)} all-to-all(bf16[8,64,256]{2,1,0:T(8,128)(2,1)S(1)} %broadcast_in_dim.44), channel_id=1, replica_groups=mesh['grp'=2,'kv'=16,'x'=8,'core'=2] {'x'}, dimensions={0} | all-to-all | bytes 524288 | tf_op jit(solution)/shard_map/all_to_all | solution.py:17
  174.1 10.3 %all_to_all.37 = bf16[2,64,256]{2,1,0:T(8,128)(2,1)S(1)} all-to-all(bf16[2,64,256]{2,1,0:T(8,128)(2,1)S(1)} %broadcast_in_dim.74), channel_id=1, replica_groups=mesh['grp'=2,'kv'=16,'x'=8,'core'=2] {'core'}, dimensions={0} | all-to-all | bytes 131072 | tf_op jit(solution)/shard_map/all_to_all | solution.py:17
  184.5 0.7 reshape.204
  (87 shorter events, 5.9 us)
Async XLA Ops:
  0.0 69.8 %copy-start = (bf16[8,256,256]{2,1,0:T(8,128)(2,1)S(1)}, bf16[8,256,256]{2,1,0:T(8,128)(2,1)}, u32[]{:S(2)}) copy-start(bf16[8,256,256]{2,1,0:T(8,128)(2,1)} %param.22) | copy-start | bytes 3145732
  0.0 1.3 copy-start.2
  0.0 54.4 %copy-start.1 = (f32[8,128,256]{2,1,0:T(8,128)S(1)}, f32[8,128,256]{2,1,0:T(8,128)}, u32[]{:S(2)}) copy-start(f32[8,128,256]{2,1,0:T(8,128)} %param.23) | copy-start | bytes 3145732
  6.8 1.8 copy-start.8
  6.8 1.8 copy-start.9
  10.0 44.4 %copy-start.13 = (s32[8]{0:T(128)S(1)}, s32[8]{0:T(128)}, u32[]{:S(2)}) copy-start(s32[8]{0:T(128)} %param.19) | copy-start | bytes 100
  10.0 57.9 %all-to-all-start = ((bf16[16,8,1024]{2,1,0:T(8,128)(2,1)}), bf16[16,8,1024]{2,1,0:T(8,128)(2,1)S(1)}, u32[]{:S(2)}, u32[]{:S(2)}) async-start(bf16[16,8,1024]{2,1,0:T(8,128)(2,1)} %bitcast.1), calls=%async_computation | async-start | bytes 524288 | tf_op jit(solution)/shard_map/all_to_all | solution.py:17
  54.4 14.9 %copy-start.3 = (bf16[8,128,256]{2,1,0:T(8,128)(2,1)S(1)}, bf16[8,128,256]{2,1,0:T(8,128)(2,1)}, u32[]{:S(2)}) copy-start(bf16[8,128,256]{2,1,0:T(8,128)(2,1)} %param.21) | copy-start | bytes 1572868
  68.2 0.7 copy-start.12
  69.8 1.0 copy-start.4
  71.5 0.7 copy-start.11
  72.3 12.5 %copy-start.7 = (bf16[256,256]{1,0:T(8,128)(2,1)S(1)}, bf16[256,256]{1,0:T(8,128)(2,1)}, u32[]{:S(2)}) copy-start(bf16[256,256]{1,0:T(8,128)(2,1)} %param.32) | copy-start | bytes 393220
  73.1 24.4 %all-to-all-start.1 = ((bf16[32,4,256]{2,1,0:T(4,128)(2,1)}), bf16[32,4,256]{2,1,0:T(4,128)(2,1)S(1)}, u32[]{:S(2)}, u32[]{:S(2)}) async-start(bf16[32,4,256]{2,1,0:T(4,128)(2,1)} %bitcast.12), calls=%async_computation.1 | async-start | bytes 131072 | tf_op jit(solution)/shard_map/all_to_all | solution.py:17
  84.7 12.8 %collective-permute-start = (bf16[256,256]{1,0:T(8,128)(2,1)S(1)}, bf16[256,256]{1,0:T(8,128)(2,1)S(1)}, u32[]{:S(2)}, u32[]{:S(2)}) collective-permute-start(bf16[256,256]{1,0:T(8,128)(2,1)S(1)} %copy-done.7), channel_id=1, source_target_pairs={{0,1},{1,0},{2,3},{3,2},{4,5},{5,4},{6,7},{7,6},{8,9},{9,8},{10,11... | collective-permute-start | bytes 393224 | tf_op jit(solution)/shard_map/ppermute | solution.py:76
  97.7 7.9 %copy-start.5 = (bf16[256,1024]{1,0:T(8,128)(2,1)S(1)}, bf16[256,1024]{1,0:T(8,128)(2,1)}, u32[]{:S(2)}) copy-start(bf16[256,1024]{1,0:T(8,128)(2,1)} %param.34) | copy-start | bytes 1572868
  98.6 16.3 %all-to-all-start.2 = ((bf16[8,64,256]{2,1,0:T(8,128)(2,1)}), bf16[8,64,256]{2,1,0:T(8,128)(2,1)S(1)}, u32[]{:S(2)}, u32[]{:S(2)}) async-start(bf16[8,64,256]{2,1,0:T(8,128)(2,1)} %broadcast_in_dim.42), calls=%async_computation.2 | async-start | bytes 524288 | tf_op jit(solution)/shard_map/all_to_all | solution.py:17
  105.7 10.6 %collective-permute-start.1 = (bf16[256,1024]{1,0:T(8,128)(2,1)S(1)}, bf16[256,1024]{1,0:T(8,128)(2,1)S(1)}, u32[]{:S(2)}, u32[]{:S(2)}) collective-permute-start(bf16[256,1024]{1,0:T(8,128)(2,1)S(1)} %copy-done.5), channel_id=1, source_target_pairs={{0,1},{1,0},{2,3},{3,2},{4,5},{5,4},{6,7},{7,6},{8,9},{9,8},{10,11... | collective-permute-start | bytes 1572872 | tf_op jit(solution)/shard_map/ppermute | solution.py:77
  115.4 0.7 copy-start.10
  135.5 12.6 %copy-start.6 = (bf16[1024,256]{1,0:T(8,128)(2,1)S(1)}, bf16[1024,256]{1,0:T(8,128)(2,1)}, u32[]{:S(2)}) copy-start(bf16[1024,256]{1,0:T(8,128)(2,1)} %param.35) | copy-start | bytes 1572868
  136.7 25.0 %all-to-all-start.4 = ((bf16[16,4,2048]{2,1,0:T(4,128)(2,1)}), bf16[16,4,2048]{2,1,0:T(4,128)(2,1)S(1)}, u32[]{:S(2)}, u32[]{:S(2)}) async-start(bf16[16,4,2048]{2,1,0:T(4,128)(2,1)} %broadcast_in_dim.43), calls=%async_computation.4 | async-start | bytes 524288 | tf_op jit(solution)/shard_map/all_to_all | solution.py:17
  148.1 13.8 %collective-permute-start.2 = (bf16[1024,256]{1,0:T(8,128)(2,1)S(1)}, bf16[1024,256]{1,0:T(8,128)(2,1)S(1)}, u32[]{:S(2)}, u32[]{:S(2)}) collective-permute-start(bf16[1024,256]{1,0:T(8,128)(2,1)S(1)} %copy-done.6), channel_id=1, source_target_pairs={{0,1},{1,0},{2,3},{3,2},{4,5},{5,4},{6,7},{7,6},{8,9},{9,8},{10,11... | collective-permute-start | bytes 1572872 | tf_op jit(solution)/shard_map/ppermute | solution.py:78

commit v2 on v1

v2 whole, which is shorter than its diff:
```python
import jax
import jax.numpy as jnp
from jax import lax
from jax.experimental import pallas as pl
from jax.experimental.pallas import tpu as pltpu
from jax.sharding import Mesh, PartitionSpec as P

D = 4096
KEY_WIDTH = 32
DV = 64
LANES = 128
SUBLANES = 8
CORES = 2

NORM_EPS = 1e-06
DECAY_SOFTNESS = 16.0

f32, bf16 = jnp.float32, jnp.bfloat16


def exchange(pieces, axes):
    return lax.all_to_all(pieces, axes, 0, 0, tiled=True)


def to_everyone(value, axes):
    peers = lax.axis_size(axes)
    return exchange(jnp.broadcast_to(value[None], (peers, *value.shape)), axes)


def dot(a, b):
    return jnp.dot(a, b, preferred_element_type=f32)


def square_lanes(square):
    high = lax.reduce_precision(square, 8, 7)
    lane = lax.broadcasted_iota(jnp.int32, (square.shape[0], LANES), 1)
    return jnp.where(lane == 0, high, jnp.where(lane == 1, square - high, 0.0)).astype(bf16)


def project_kernel(tokens, gain, *refs):
    *weights, out = refs
    rows = tokens[...].astype(f32)
    square = jnp.sum(rows * rows, axis=1, keepdims=True)
    scaled = (rows * gain[...]).astype(bf16)
    start = 0
    for w in weights:
        width = w.shape[1]
        out[:, start : start + width] = dot(scaled, w[...]).astype(bf16)
        start += width
    high = square.astype(bf16).astype(f32)
    lane = lax.broadcasted_iota(jnp.int32, (rows.shape[0], LANES), 1)
    out[:, start:] = jnp.where(lane == 0, high, jnp.where(lane == 1, square - high, 0.0)).astype(
        bf16
    )


def project(tokens, gain, weights):
    width = sum(w.shape[1] for w in weights) + LANES
    return pl.pallas_call(
        project_kernel,
        out_shape=jax.ShapeDtypeStruct((tokens.shape[0], width), bf16),
        name="project",
    )(tokens, gain.reshape(1, -1), *weights)


def span_kernel(lengths, keys, decays, weighted, start_factor, columns):
    seq_count, channels, span = keys.shape
    place = lax.broadcasted_iota(jnp.int32, (1, span), 1)
    for n in range(seq_count):
        length = lengths[n]
        decay = decays[n]
        last = jnp.sum(jnp.where(place == length - 2, decay, 0.0), axis=1, keepdims=True)
        factor = jnp.where(place < length - 1, jnp.exp(last - decay), 0.0)
        weighted[n] = keys[n].astype(f32) * factor
        columns[:, n : n + 1] = last
    start_factor[...] = jnp.exp(columns[...].T)[:seq_count]


def span_terms(lengths, keys, decays):
    seq_count, channels, span = keys.shape
    vmem = pl.BlockSpec(memory_space=pltpu.VMEM)
    return pl.pallas_call(
        span_kernel,
        in_specs=[pl.BlockSpec(memory_space=pltpu.SMEM), vmem, vmem],
        out_shape=(
            jax.ShapeDtypeStruct(keys.shape, f32),
            jax.ShapeDtypeStruct((seq_count, channels), f32),
        ),
        scratch_shapes=[pltpu.VMEM((channels, LANES), f32)],
        name="span",
    )(lengths, keys, decays)


def attend_kernel(arrived, weighted, start_factor, values, state, bias, gain, out):
    seq_count, channels = start_factor.shape
    heads = channels // KEY_WIDTH
    width = heads * DV
    total = arrived[0].astype(f32)
    for k in range(1, arrived.shape[0]):
        total += arrived[k].astype(f32)
    query_sum = total[:, :channels]
    key_sum = total[:, channels : 2 * channels]
    decay_sum = total[:, 2 * channels : 3 * channels]
    value_sum = total[:, 3 * channels : 3 * channels + width]
    gate_sum = total[:, 3 * channels + width : 3 * channels + 2 * width]
    square = jnp.sum(total[:, 3 * channels + 2 * width :], axis=1, keepdims=True)
    scale = lax.rsqrt(square / D + NORM_EPS)
    query = query_sum * scale * KEY_WIDTH ** (-0.5)
    key_new = key_sum * scale
    value_new = value_sum * scale
    gate = gate_sum * scale
    before = decay_sum * scale + bias[...]
    log_sigmoid = jnp.minimum(before, 0.0) - jnp.log1p(jnp.exp(-jnp.abs(before)))
    decayed = query * jnp.exp(log_sigmoid / DECAY_SOFTNESS)

    key_head = lax.broadcasted_iota(jnp.int32, (SUBLANES, channels), 1) // KEY_WIDTH
    key_row = lax.broadcasted_iota(jnp.int32, (SUBLANES, channels), 0)
    value_head = lax.broadcasted_iota(jnp.int32, (SUBLANES, width), 1) // DV
    value_row = lax.broadcasted_iota(jnp.int32, (SUBLANES, width), 0)
    at_start = decayed * start_factor[...]
    padded = jnp.concatenate([decayed, jnp.zeros((LANES - seq_count, channels), f32)], axis=0)
    by_channel = padded.T
    rows = []
    for n in range(seq_count):
        product = weighted[n] * by_channel[:, n : n + 1]
        scores = [
            jnp.sum(product[h * KEY_WIDTH : (h + 1) * KEY_WIDTH], axis=0, keepdims=True)
            for h in range(heads)
        ]
        scores.append(jnp.zeros((SUBLANES - heads, product.shape[1]), f32))
        low = jnp.concatenate(scores, axis=0).astype(bf16)
        history = lax.dot_general(
            low, values[n], (((1,), (1,)), ((), ())), preferred_element_type=f32
        )
        of_heads = jnp.where(key_head == key_row, at_start[n : n + 1], 0.0)
        carried = lax.dot_general(
            of_heads,
            state[n].reshape(channels, DV),
            (((1,), (0,)), ((), ())),
            precision=lax.Precision.HIGHEST,
            preferred_element_type=f32,
        )
        both = history + jnp.concatenate([carried] * heads, axis=1)
        rows.append(jnp.sum(jnp.where(value_head == value_row, both, 0.0), axis=0, keepdims=True))
    raw = jnp.concatenate(rows, axis=0)
    match = query * key_new
    own = jnp.zeros_like(raw)
    column = lax.broadcasted_iota(jnp.int32, raw.shape, 1) // DV
    channel = lax.broadcasted_iota(jnp.int32, match.shape, 1) // KEY_WIDTH
    for h in range(heads):
        amount = jnp.sum(jnp.where(channel == h, match, 0.0), axis=1, keepdims=True)
        own = jnp.where(column == h, amount, own)
    raw = raw + own * value_new
    power = raw * raw
    inverse = jnp.zeros_like(raw)
    for h in range(heads):
        mean = jnp.sum(jnp.where(column == h, power, 0.0), axis=1, keepdims=True) / DV
        inverse = jnp.where(column == h, lax.rsqrt(mean + NORM_EPS), inverse)
    mixed = raw * inverse * gain[...] * (gate * jax.nn.sigmoid(gate))
    half = seq_count // CORES
    low = mixed.astype(bf16)
    for c in range(CORES):
        piece = low[c * half : (c + 1) * half]
        for k in range(out.shape[0] // CORES):
            out[k * CORES + c] = piece


def attend(arrived, weighted, start_factor, values, state, bias, gain):
    seq_count, width = values.shape[:2]
    half = seq_count // CORES
    return pl.pallas_call(
        attend_kernel,
        out_shape=jax.ShapeDtypeStruct((arrived.shape[0] * CORES, half, width), bf16),
        name="attend",
    )(arrived, weighted, start_factor, values, state, bias, gain)


def shards(
    tokens,
    span_lengths,
    block_state,
    key_cache,
    value_cache,
    decay_cache,
    attn_gain,
    query_weight,
    key_weight,
    value_weight,
    gate_weight,
    decay_matrix,
    decay_offset_bias,
    head_gain,
    out_weight,
    mixer_gain,
    up_weight,
    down_weight,
):
    seq_count, head_count = block_state.shape[:2]
    peers = lax.axis_size("kv")
    core = lax.axis_index("core")
    half = seq_count // CORES
    rows_half = peers * half
    values = head_count * DV

    sent = project(
        tokens, attn_gain, (query_weight, key_weight, decay_matrix, value_weight, gate_weight)
    )
    arrived = exchange(sent.reshape(peers, seq_count, -1), "kv")

    swap = [(c, CORES - 1 - c) for c in range(CORES)]
    out_other = lax.ppermute(out_weight, "core", swap)
    up_other = lax.ppermute(up_weight, "core", swap)
    down_other = lax.ppermute(down_weight, "core", swap)
    out_first = jnp.where(core == 0, out_weight, out_other)
    out_second = jnp.where(core == 0, out_other, out_weight)
    own_tokens = lax.dynamic_index_in_dim(
        tokens.reshape(peers, CORES, half, -1), core, 1, keepdims=False
    ).reshape(rows_half, -1)
    weighted, start_factor = span_terms(span_lengths, key_cache, decay_cache)
    gain = jnp.tile(head_gain, head_count).reshape(1, -1)
    (
        arrived,
        out_first,
        out_second,
        up_other,
        down_other,
        own_tokens,
        weighted,
        start_factor,
        gain,
    ) = lax.optimization_barrier(
        (
            arrived,
            out_first,
            out_second,
            up_other,
            down_other,
            own_tokens,
            weighted,
            start_factor,
            gain,
        )
    )

    spread = attend(
        arrived,
        weighted,
        start_factor,
        value_cache,
        block_state,
        decay_offset_bias.reshape(1, -1),
        gain,
    )
    heads = exchange(spread, ("kv", "core")).reshape(peers, CORES, half, values)
    attn_terms = dot(heads[:, 0].reshape(rows_half, values), out_first) + dot(
        heads[:, 1].reshape(rows_half, values), out_second
    )
    attn_out = jnp.sum(to_everyone(attn_terms.astype(bf16), "x").astype(f32), axis=0)
    resid = (own_tokens.astype(f32) + attn_out).astype(bf16)
    resid_rows = resid.astype(f32)
    mixer_square = jnp.sum(resid_rows * resid_rows, axis=1, keepdims=True)
    mixer_scaled = (resid_rows * mixer_gain).astype(bf16)
    up_sent = jnp.concatenate(
        [
            dot(mixer_scaled, up_weight).astype(bf16),
            dot(mixer_scaled, up_other).astype(bf16),
            square_lanes(mixer_square),
        ],
        axis=1,
    )
    up_total = jnp.sum(exchange(up_sent.reshape(peers, half, -1), "kv").astype(f32), axis=0)
    hidden_count = up_weight.shape[1] * CORES
    before, squares = up_total[:, :hidden_count], up_total[:, hidden_count:]
    mixer_scale = lax.rsqrt((squares[:, :1] + squares[:, 1:2]) / D + NORM_EPS)
    hidden = jnp.square(jax.nn.relu(before * mixer_scale)).astype(bf16)
    every = to_everyone(hidden, "kv").reshape(rows_half, hidden_count)
    own_count = up_weight.shape[1]
    down_terms = dot(every[:, :own_count], down_weight) + dot(every[:, own_count:], down_other)
    mixer_out = jnp.sum(to_everyone(down_terms.astype(bf16), "x").astype(f32), axis=0)
    own_out = (resid_rows + mixer_out).astype(bf16)
    both = to_everyone(own_out, "core").reshape(CORES, peers, half, -1)
    return jnp.swapaxes(both, 0, 1).reshape(peers * seq_count, -1)


def solution(mesh):
    sizes = dict(mesh.shape)
    fine = Mesh(
        mesh.devices.reshape(sizes["grp"], sizes["kv"], sizes["tp"] // CORES, CORES),
        ("grp", "kv", "x", "core"),
    )
    tp = ("x", "core")
    placed = (
        P("grp", "kv"),
        P(("grp", "kv")),
        P(("grp", "kv"), tp, None, None),
        P(("grp", "kv"), tp, None),
        P(("grp", "kv"), tp, None),
        P(("grp", "kv"), tp, None),
        P("kv"),
        P("kv", tp),
        P("kv", tp),
        P("kv", tp),
        P("kv", tp),
        P("kv", tp),
        P(tp),
        P(),
        P(tp, "kv"),
        P("kv"),
        P("kv", tp),
        P(tp, "kv"),
    )
    return jax.shard_map(
        shards, mesh=fine, in_specs=placed, out_specs=P("grp", "kv"), check_vma=False
    )
```

time: 186 us -> 176 us (0.946)
  blocking collectives: 41 us -> 90.2 us
  waiting for transfers between devices: 39.3 us -> 11.2 us
  starting transfers between devices: 83.8 us -> 58.9 us
  Pallas kernels: 0 us -> 8.47 us
  matrix products: 7.84 us -> 1.13 us
  local copies, waits for them, and re-layouts: 9.41 us -> 4.52 us
  other arithmetic: 3.4 us -> 0.74 us
    all_to_all x3 -> x5, blocking collectives: 41 us -> 90.2 us  [exchange(): return lax.all_to_all(pieces, axes, 0, 0, tiled=True)]
    all_to_all x4 -> x2, waiting for transfers between devices: 39.3 us -> 11.2 us  [exchange(): return lax.all_to_all(pieces, axes, 0, 0, tiled=True)]
    all_to_all x4 -> x2, starting transfers between devices: 74.4 us -> 51.4 us  [exchange(): return lax.all_to_all(pieces, axes, 0, 0, tiled=True)]
    pallas_call x0 -> x3, Pallas kernels: none -> 8.47 us  [the longest x1 3.67 us: attend(): pl.pallas_call(attend_kernel, out_shape=jax.ShapeDtypeStruct((arrived.sha...]
    dot_general x13 -> x6, matrix products: 7.84 us -> 1.13 us  [dot(): return jnp.dot(a, b, preferred_element_type=f32)]
    unnamed x31 -> x15, local copies, waits for them, and re-layouts: 4.48 us -> 2.03 us
    reduce_sum x5 -> x0, other arithmetic: 1.96 us -> none  [the longest x1 1.09 us: shards(): square_sum = jnp.sum(whole_rows * whole_rows, axis=1, keepdims=True)]
  transfers between devices with their start and end apart: 7 -> 5, of which waited for: 4 -> 2; matrix products, arithmetic and copies ran while one was open for 1% -> 0% of each run, Pallas kernels for 0% -> 2%
where the time goes in v2:
time: 176 us; the launch traced here: 175 us
  blocking collectives  90.2 us (51%)
  starting transfers between devices  58.9 us (33%)
  waiting for transfers between devices  11.2 us (6%)
  Pallas kernels  8.47 us (5%)
  local copies, waits for them, and re-layouts  4.52 us (3%)
    all_to_all x5, blocking collectives, exchange(): return lax.all_to_all(pieces, axes, 0, 0, tiled=True)  90.2 us
    all_to_all x2, starting transfers between devices, exchange(): return lax.all_to_all(pieces, axes, 0, 0, tiled=True)  51.4 us
    all_to_all x2, waiting for transfers between devices, exchange(): return lax.all_to_all(pieces, axes, 0, 0, tiled=True)  11.2 us
    pallas_call x1, Pallas kernels, attend(): pl.pallas_call(attend_kernel, out_shape=jax.ShapeDtypeStruct((arrived.sha...  3.67 us
  transfers between devices with their start and end apart: 5, of which 2 were waited for; matrix products, arithmetic and copies ran while one was open for 0% of the time, Pallas kernels for 2%

profile of v2, /device:TPU:65, one launch (start us, length us, event | category | flops | bytes accessed | tf_op | source)
XLA Modules:
  0.0 175.4 jit_solution(10784828607252697841)
XLA Ops:
  0.0 2.1 %project.1 = bf16[128,1024]{1,0:T(8,128)(2,1)} custom-call(bf16[128,256]{1,0:T(8,128)(2,1)} %tokens.1, f32[1,256]{1,0:T(1,128)} %bitcast.22, bf16[256,128]{1,0:T(8,128)(2,1)} %refs_0_.1, bf16[256,128]{1,0:T(8,128)(2,1)} %refs_1_.1, bf16[256,128]{1,0:T(8,128)(2,1)} %refs_2_.1, bf16[256,256]{1,0:T(8,128)(2,1)} %refs_3_.1, bf16[256,256]{1,0:T(8,128)(2,1)} %refs_4_.1), custom_call_target="tpu_custom_call" | custom-call | tf_op jit(solution)/shard_map/project/pallas_call | solution.py:59
  2.1 44.4 %all-to-all-start = ((bf16[16,8,1024]{2,1,0:T(8,128)(2,1)}), bf16[16,8,1024]{2,1,0:T(8,128)(2,1)S(1)}, u32[]{:S(2)}, u32[]{:S(2)}) async-start(bf16[16,8,1024]{2,1,0:T(8,128)(2,1)} %bitcast.19), calls=%async_computation | async-start | bytes 524288 | tf_op jit(solution)/shard_map/all_to_all | solution.py:22
  46.5 3.1 %collective-permute-start.1 = (bf16[256,1024]{1,0:T(8,128)(2,1)S(1)}, bf16[256,1024]{1,0:T(8,128)(2,1)S(1)}, u32[]{:S(2)}, u32[]{:S(2)}) collective-permute-start(bf16[256,1024]{1,0:T(8,128)(2,1)S(1)} %copy-done.1), channel_id=1, source_target_pairs={{0,1},{1,0},{2,3},{3,2},{4,5},{5,4},{6,7},{7,6},{8,9},{9,8},{10,11... | collective-permute-start | bytes 1572872 | tf_op jit(solution)/shard_map/ppermute | solution.py:212
  49.6 2.0 %collective-permute-start.2 = (bf16[1024,256]{1,0:T(8,128)(2,1)S(1)}, bf16[1024,256]{1,0:T(8,128)(2,1)S(1)}, u32[]{:S(2)}, u32[]{:S(2)}) collective-permute-start(bf16[1024,256]{1,0:T(8,128)(2,1)S(1)} %copy-done.2), channel_id=1, source_target_pairs={{0,1},{1,0},{2,3},{3,2},{4,5},{5,4},{6,7},{7,6},{8,9},{9,8},{10,11... | collective-permute-start | bytes 1572872 | tf_op jit(solution)/shard_map/ppermute | solution.py:213
  51.6 2.4 %collective-permute-start = (bf16[256,256]{1,0:T(8,128)(2,1)S(1)}, bf16[256,256]{1,0:T(8,128)(2,1)S(1)}, u32[]{:S(2)}, u32[]{:S(2)}) collective-permute-start(bf16[256,256]{1,0:T(8,128)(2,1)S(1)} %copy-done.4), channel_id=1, source_target_pairs={{0,1},{1,0},{2,3},{3,2},{4,5},{5,4},{6,7},{7,6},{8,9},{9,8},{10,11... | collective-permute-start | bytes 393224 | tf_op jit(solution)/shard_map/ppermute | solution.py:211
  54.2 0.6 copy-done.6
  54.8 0.7 reshape_tile.3.gain
  55.4 2.7 %span.1 = (f32[8,128,256]{2,1,0:T(8,128)}, f32[8,128]{1,0:T(8,128)}) custom-call(s32[8]{0:T(128)} %lengths.1, bf16[8,128,256]{2,1,0:T(8,128)(2,1)} %keys.1, f32[8,128,256]{2,1,0:T(8,128)} %decays.1), custom_call_target="tpu_custom_call" | custom-call | tf_op jit(solution)/shard_map/span/pallas_call | solution.py:82
  58.2 1.9 %all-to-all-done.arrived = bf16[16,8,1024]{2,1,0:T(8,128)(2,1)S(1)} async-done(((bf16[16,8,1024]{2,1,0:T(8,128)(2,1)}), bf16[16,8,1024]{2,1,0:T(8,128)(2,1)S(1)}, u32[]{:S(2)}, u32[]{:S(2)}) %all-to-all-start) | async-done | bytes 262176 | tf_op jit(solution)/shard_map/all_to_all | solution.py:22
  60.1 0.7 copy-done
  60.8 3.7 %attend.1 = bf16[32,4,256]{2,1,0:T(4,128)(2,1)} custom-call(bf16[16,8,1024]{2,1,0:T(8,128)(2,1)} %copy-done, f32[8,128,256]{2,1,0:T(8,128)} %get-tuple-element.20.weighted, f32[8,128]{1,0:T(8,128)} %get-tuple-element.21.start_factor, bf16[8,256,256]{2,1,0:T(8,128)(2,1)} %values.1, f32[8,4,32,64]{3,2,1,0:T(8,128)} %state.1, f32[1,128]{1,0:T(1,128)} %bitcast.23, ...), custom_call_target="tpu_custom_call" | custom-call | tf_op jit(solution)/shard_map/attend/pallas_call | solution.py:171
  64.4 24.4 %all_to_all.35 = bf16[32,4,256]{2,1,0:T(4,128)(2,1)S(1)} all-to-all(bf16[32,4,256]{2,1,0:T(4,128)(2,1)} %attend.1), channel_id=1, replica_groups=mesh['grp'=2,'kv'=16,'x'=8,'core'=2] {'kv','core'}, dimensions={0} | all-to-all | bytes 131072 | tf_op jit(solution)/shard_map/all_to_all | solution.py:22
  88.9 0.1 fusion.19
  89.0 0.2 fusion
  89.2 0.7 broadcast_in_dim.28
  89.9 7.0 %all-to-all-start.2 = ((bf16[8,64,256]{2,1,0:T(8,128)(2,1)}), bf16[8,64,256]{2,1,0:T(8,128)(2,1)S(1)}, u32[]{:S(2)}, u32[]{:S(2)}) async-start(bf16[8,64,256]{2,1,0:T(8,128)(2,1)} %broadcast_in_dim.28), calls=%async_computation.2 | async-start | bytes 524288 | tf_op jit(solution)/shard_map/all_to_all | solution.py:22
  97.0 9.3 %all-to-all-done.2 = bf16[8,64,256]{2,1,0:T(8,128)(2,1)S(1)} async-done(((bf16[8,64,256]{2,1,0:T(8,128)(2,1)}), bf16[8,64,256]{2,1,0:T(8,128)(2,1)S(1)}, u32[]{:S(2)}, u32[]{:S(2)}) %all-to-all-start.2) | async-done | bytes 262176 | tf_op jit(solution)/shard_map/all_to_all | solution.py:22
  106.3 0.1 fusion.6
  106.4 0.7 copy-done.5
  107.1 0.2 convolution_convert_fusion.1
  107.3 0.2 convolution_convert_fusion
  107.7 18.9 %all_to_all.36 = bf16[16,4,2176]{2,1,0:T(4,128)(2,1)S(1)} all-to-all(bf16[16,4,2176]{2,1,0:T(4,128)(2,1)S(1)} %reshape.51), channel_id=1, replica_groups=mesh['grp'=2,'kv'=16,'x'=8,'core'=2] {'kv'}, dimensions={0} | all-to-all | bytes 557056 | tf_op jit(solution)/shard_map/all_to_all | solution.py:22
  126.6 0.1 convert_reduce_fusion
  126.8 0.2 fusion.16
  127.0 0.1 fusion.10
  127.0 0.1 broadcast_in_dim.50
  127.2 24.8 %all_to_all.37 = bf16[16,4,2048]{2,1,0:T(4,128)(2,1)S(1)} all-to-all(bf16[16,4,2048]{2,1,0:T(4,128)(2,1)S(1)} %broadcast_in_dim.50), channel_id=1, replica_groups=mesh['grp'=2,'kv'=16,'x'=8,'core'=2] {'kv'}, dimensions={0} | all-to-all | bytes 524288 | tf_op jit(solution)/shard_map/all_to_all | solution.py:22
  152.0 0.2 fusion.3
  152.2 0.2 fusion.1
  152.4 11.8 %all_to_all.38 = bf16[8,64,256]{2,1,0:T(8,128)(2,1)S(1)} all-to-all(bf16[8,64,256]{2,1,0:T(8,128)(2,1)S(1)} %broadcast_in_dim.51), channel_id=1, replica_groups=mesh['grp'=2,'kv'=16,'x'=8,'core'=2] {'x'}, dimensions={0} | all-to-all | bytes 524288 | tf_op jit(solution)/shard_map/all_to_all | solution.py:22
  164.3 10.3 %all_to_all.39 = bf16[2,64,256]{2,1,0:T(8,128)(2,1)S(1)} all-to-all(bf16[2,64,256]{2,1,0:T(8,128)(2,1)S(1)} %broadcast_in_dim.52), channel_id=1, replica_groups=mesh['grp'=2,'kv'=16,'x'=8,'core'=2] {'core'}, dimensions={0} | all-to-all | bytes 131072 | tf_op jit(solution)/shard_map/all_to_all | solution.py:22
  174.8 0.7 reshape.54
  (35 shorter events, 0.6 us)
Async XLA Ops:
  0.0 46.5 %copy-start.1 = (bf16[256,1024]{1,0:T(8,128)(2,1)S(1)}, bf16[256,1024]{1,0:T(8,128)(2,1)}, u32[]{:S(2)}) copy-start(bf16[256,1024]{1,0:T(8,128)(2,1)} %param.34) | copy-start | bytes 1572868
  0.0 49.6 %copy-start.2 = (bf16[1024,256]{1,0:T(8,128)(2,1)S(1)}, bf16[1024,256]{1,0:T(8,128)(2,1)}, u32[]{:S(2)}) copy-start(bf16[1024,256]{1,0:T(8,128)(2,1)} %param.35) | copy-start | bytes 1572868
  2.1 49.5 %copy-start.4 = (bf16[256,256]{1,0:T(8,128)(2,1)S(1)}, bf16[256,256]{1,0:T(8,128)(2,1)}, u32[]{:S(2)}) copy-start(bf16[256,256]{1,0:T(8,128)(2,1)} %param.32) | copy-start | bytes 393220
  2.1 51.9 %copy-start.3 = (bf16[128,256]{1,0:T(8,128)(2,1)S(1)}, bf16[128,256]{1,0:T(8,128)(2,1)}, u32[]{:S(2)}) copy-start(bf16[128,256]{1,0:T(8,128)(2,1)} %tokens.1) | copy-start | bytes 196612
  2.1 57.9 %all-to-all-start = ((bf16[16,8,1024]{2,1,0:T(8,128)(2,1)}), bf16[16,8,1024]{2,1,0:T(8,128)(2,1)S(1)}, u32[]{:S(2)}, u32[]{:S(2)}) async-start(bf16[16,8,1024]{2,1,0:T(8,128)(2,1)} %bitcast.19), calls=%async_computation | async-start | bytes 524288 | tf_op jit(solution)/shard_map/all_to_all | solution.py:22
  46.5 11.7 %collective-permute-start.1 = (bf16[256,1024]{1,0:T(8,128)(2,1)S(1)}, bf16[256,1024]{1,0:T(8,128)(2,1)S(1)}, u32[]{:S(2)}, u32[]{:S(2)}) collective-permute-start(bf16[256,1024]{1,0:T(8,128)(2,1)S(1)} %copy-done.1), channel_id=1, source_target_pairs={{0,1},{1,0},{2,3},{3,2},{4,5},{5,4},{6,7},{7,6},{8,9},{9,8},{10,11... | collective-permute-start | bytes 1572872 | tf_op jit(solution)/shard_map/ppermute | solution.py:212
  49.6 8.5 %collective-permute-start.2 = (bf16[1024,256]{1,0:T(8,128)(2,1)S(1)}, bf16[1024,256]{1,0:T(8,128)(2,1)S(1)}, u32[]{:S(2)}, u32[]{:S(2)}) collective-permute-start(bf16[1024,256]{1,0:T(8,128)(2,1)S(1)} %copy-done.2), channel_id=1, source_target_pairs={{0,1},{1,0},{2,3},{3,2},{4,5},{5,4},{6,7},{7,6},{8,9},{9,8},{10,11... | collective-permute-start | bytes 1572872 | tf_op jit(solution)/shard_map/ppermute | solution.py:213
  51.6 6.5 %collective-permute-start = (bf16[256,256]{1,0:T(8,128)(2,1)S(1)}, bf16[256,256]{1,0:T(8,128)(2,1)S(1)}, u32[]{:S(2)}, u32[]{:S(2)}) collective-permute-start(bf16[256,256]{1,0:T(8,128)(2,1)S(1)} %copy-done.4), channel_id=1, source_target_pairs={{0,1},{1,0},{2,3},{3,2},{4,5},{5,4},{6,7},{7,6},{8,9},{9,8},{10,11... | collective-permute-start | bytes 393224 | tf_op jit(solution)/shard_map/ppermute | solution.py:211
  54.1 0.7 copy-start.6
  60.1 0.7 copy-start
  89.9 16.3 %all-to-all-start.2 = ((bf16[8,64,256]{2,1,0:T(8,128)(2,1)}), bf16[8,64,256]{2,1,0:T(8,128)(2,1)S(1)}, u32[]{:S(2)}, u32[]{:S(2)}) async-start(bf16[8,64,256]{2,1,0:T(8,128)(2,1)} %broadcast_in_dim.28), calls=%async_computation.2 | async-start | bytes 524288 | tf_op jit(solution)/shard_map/all_to_all | solution.py:22
  106.4 0.7 copy-start.5

commit v3 on v2

--- a/solution.py
+++ b/solution.py
@@ -27,14 +27,15 @@
     return exchange(jnp.broadcast_to(value[None], (peers, *value.shape)), axes)
 
 
+def in_vmem(*values):
+    return tuple(pltpu.with_memory_space_constraint(v, pltpu.VMEM) for v in values)
+
+
+VMEM = pl.BlockSpec(memory_space=pltpu.VMEM)
+
+
 def dot(a, b):
     return jnp.dot(a, b, preferred_element_type=f32)
-
-
-def square_lanes(square):
-    high = lax.reduce_precision(square, 8, 7)
-    lane = lax.broadcasted_iota(jnp.int32, (square.shape[0], LANES), 1)
-    return jnp.where(lane == 0, high, jnp.where(lane == 1, square - high, 0.0)).astype(bf16)
 
 
 def project_kernel(tokens, gain, *refs):
@@ -63,7 +64,15 @@
     )(tokens, gain.reshape(1, -1), *weights)
 
 
-def span_kernel(lengths, keys, decays, weighted, start_factor, columns):
+def span_kernel(
+    lengths, keys, decays, head_gain, bias, wide_gain, weighted, start_factor, *small_and_columns
+):
+    head_gain_out, bias_out, wide_gain_out, columns = small_and_columns
+    head_gain_out[...] = jnp.concatenate(
+        [head_gain[...]] * (head_gain_out.shape[1] // head_gain.shape[1]), axis=1
+    )
+    bias_out[...] = bias[...]
+    wide_gain_out[...] = wide_gain[...]
     seq_count, channels, span = keys.shape
     place = lax.broadcasted_iota(jnp.int32, (1, span), 1)
     for n in range(seq_count):
@@ -76,22 +85,27 @@
     start_factor[...] = jnp.exp(columns[...].T)[:seq_count]
 
 
-def span_terms(lengths, keys, decays):
+def span_terms(lengths, keys, decays, head_gain, bias, wide_gain):
     seq_count, channels, span = keys.shape
-    vmem = pl.BlockSpec(memory_space=pltpu.VMEM)
+    values = channels // KEY_WIDTH * DV
     return pl.pallas_call(
         span_kernel,
-        in_specs=[pl.BlockSpec(memory_space=pltpu.SMEM), vmem, vmem],
+        in_specs=[pl.BlockSpec(memory_space=pltpu.SMEM)] + [VMEM] * 5,
+        out_specs=(VMEM,) * 5,
         out_shape=(
-            jax.ShapeDtypeStruct(keys.shape, f32),
-            jax.ShapeDtypeStruct((seq_count, channels), f32),
+            pltpu.VMEM(keys.shape, f32),
+            pltpu.VMEM((seq_count, channels), f32),
+            pltpu.VMEM((1, values), f32),
+            pltpu.VMEM((1, channels), f32),
+            pltpu.VMEM((1, wide_gain.shape[0]), f32),
         ),
         scratch_shapes=[pltpu.VMEM((channels, LANES), f32)],
+        compiler_params=pltpu.CompilerParams(vmem_limit_bytes=16 << 20),
         name="span",
-    )(lengths, keys, decays)
-
-
-def attend_kernel(arrived, weighted, start_factor, values, state, bias, gain, out):
+    )(lengths, keys, decays, *(v.reshape(1, -1) for v in (head_gain, bias, wide_gain)))
+
+
+def attend_kernel(arrived, weighted, start_factor, bias, gain, values, state, out):
     seq_count, channels = start_factor.shape
     heads = channels // KEY_WIDTH
     width = heads * DV
@@ -170,9 +184,56 @@
     half = seq_count // CORES
     return pl.pallas_call(
         attend_kernel,
-        out_shape=jax.ShapeDtypeStruct((arrived.shape[0] * CORES, half, width), bf16),
+        in_specs=[VMEM] * 7,
+        out_specs=VMEM,
+        out_shape=pltpu.VMEM((arrived.shape[0] * CORES, half, width), bf16),
+        compiler_params=pltpu.CompilerParams(vmem_limit_bytes=16 << 20),
         name="attend",
-    )(arrived, weighted, start_factor, values, state, bias, gain)
+    )(*in_vmem(arrived, weighted, start_factor, bias, gain, values, state))
+
+
+def hidden_kernel(arrived, tokens, gain, first, second_far, out, resid, second, done):
+    copy = pltpu.make_async_copy(second_far, second, done)
+    copy.start()
+    total = arrived[0].astype(f32)
+    for x in range(1, arrived.shape[0]):
+        total += arrived[x].astype(f32)
+    low = (tokens[...].astype(f32) + total).astype(bf16)
+    resid[...] = low
+    rows = low.astype(f32)
+    square = jnp.sum(rows * rows, axis=1, keepdims=True)
+    scaled = (rows * gain[...]).astype(bf16)
+    own = first.shape[1]
+    high = square.astype(bf16).astype(f32)
+    lane = lax.broadcasted_iota(jnp.int32, (rows.shape[0], LANES), 1)
+    squares = jnp.where(lane == 0, high, jnp.where(lane == 1, square - high, 0.0)).astype(bf16)
+    pieces, half = out.shape[:2]
+
+
+    def put(at, value):
+        for k in range(pieces):
+            out[k, :, at : at + value.shape[1]] = value[k * half : (k + 1) * half]
+
+    put(0, dot(scaled, first[...]).astype(bf16))
+    put(2 * own, squares)
+    copy.wait()
+    put(own, dot(scaled, second[...]).astype(bf16))
+
+
+def hidden_terms(arrived, tokens, gain, first, second, peers):
+    rows, width = tokens.shape
+    return pl.pallas_call(
+        hidden_kernel,
+        in_specs=[VMEM] * 4 + [pl.BlockSpec(memory_space=pl.ANY)],
+        out_specs=(VMEM, VMEM),
+        out_shape=(
+            pltpu.VMEM((peers, rows // peers, 2 * first.shape[1] + LANES), bf16),
+            pltpu.VMEM((rows, width), bf16),
+        ),
+        scratch_shapes=[pltpu.VMEM(second.shape, second.dtype), pltpu.SemaphoreType.DMA(())],
+        compiler_params=pltpu.CompilerParams(vmem_limit_bytes=16 << 20),
+        name="hidden",
+    )(*in_vmem(arrived, tokens, gain, first), second)
 
 
 def shards(
@@ -216,59 +277,26 @@
     own_tokens = lax.dynamic_index_in_dim(
         tokens.reshape(peers, CORES, half, -1), core, 1, keepdims=False
     ).reshape(rows_half, -1)
-    weighted, start_factor = span_terms(span_lengths, key_cache, decay_cache)
-    gain = jnp.tile(head_gain, head_count).reshape(1, -1)
-    (
-        arrived,
-        out_first,
-        out_second,
-        up_other,
-        down_other,
-        own_tokens,
-        weighted,
-        start_factor,
-        gain,
-    ) = lax.optimization_barrier(
-        (
-            arrived,
-            out_first,
-            out_second,
-            up_other,
-            down_other,
-            own_tokens,
-            weighted,
-            start_factor,
-            gain,
+    ready = span_terms(
+        span_lengths, key_cache, decay_cache, head_gain, decay_offset_bias, mixer_gain
+    )
+    arrived, out_first, out_second, up_other, down_other, own_tokens, ready = (
+        lax.optimization_barrier(
+            (arrived, out_first, out_second, up_other, down_other, own_tokens, ready)
         )
     )
-
-    spread = attend(
-        arrived,
-        weighted,
-        start_factor,
-        value_cache,
-        block_state,
-        decay_offset_bias.reshape(1, -1),
-        gain,
-    )
+    weighted, start_factor, gain, bias, wide_gain = ready
+
+    spread = attend(arrived, weighted, start_factor, value_cache, block_state, bias, gain)
     heads = exchange(spread, ("kv", "core")).reshape(peers, CORES, half, values)
     attn_terms = dot(heads[:, 0].reshape(rows_half, values), out_first) + dot(
         heads[:, 1].reshape(rows_half, values), out_second
     )
-    attn_out = jnp.sum(to_everyone(attn_terms.astype(bf16), "x").astype(f32), axis=0)
-    resid = (own_tokens.astype(f32) + attn_out).astype(bf16)
-    resid_rows = resid.astype(f32)
-    mixer_square = jnp.sum(resid_rows * resid_rows, axis=1, keepdims=True)
-    mixer_scaled = (resid_rows * mixer_gain).astype(bf16)
-    up_sent = jnp.concatenate(
-        [
-            dot(mixer_scaled, up_weight).astype(bf16),
-            dot(mixer_scaled, up_other).astype(bf16),
-            square_lanes(mixer_square),
-        ],
-        axis=1,
-    )
-    up_total = jnp.sum(exchange(up_sent.reshape(peers, half, -1), "kv").astype(f32), axis=0)
+    attn_arrived = to_everyone(attn_terms.astype(bf16), "x")
+    up_sent, resid = hidden_terms(
+        attn_arrived, own_tokens, wide_gain, up_weight, up_other, peers
+    )
+    up_total = jnp.sum(exchange(up_sent, "kv").astype(f32), axis=0)
     hidden_count = up_weight.shape[1] * CORES
     before, squares = up_total[:, :hidden_count], up_total[:, hidden_count:]
     mixer_scale = lax.rsqrt((squares[:, :1] + squares[:, 1:2]) / D + NORM_EPS)
@@ -277,7 +305,7 @@
     own_count = up_weight.shape[1]
     down_terms = dot(every[:, :own_count], down_weight) + dot(every[:, own_count:], down_other)
     mixer_out = jnp.sum(to_everyone(down_terms.astype(bf16), "x").astype(f32), axis=0)
-    own_out = (resid_rows + mixer_out).astype(bf16)
+    own_out = (resid.astype(f32) + mixer_out).astype(bf16)
     both = to_everyone(own_out, "core").reshape(CORES, peers, half, -1)
     return jnp.swapaxes(both, 0, 1).reshape(peers * seq_count, -1)
 

time: 176 us -> 173 us (0.983)
  blocking collectives: 90.2 us -> 106 us
  waiting for transfers between devices: 11.2 us -> 2.23 us
  starting transfers between devices: 58.9 us -> 51.9 us
  Pallas kernels: 8.47 us -> 5.63 us
    all_to_all x5 -> x6, blocking collectives: 90.2 us -> 106 us  [exchange(): return lax.all_to_all(pieces, axes, 0, 0, tiled=True)]
    all_to_all x2 -> x1, waiting for transfers between devices: 11.2 us -> 2.22 us  [exchange(): return lax.all_to_all(pieces, axes, 0, 0, tiled=True)]
    all_to_all x2 -> x1, starting transfers between devices: 51.4 us -> 44.4 us  [exchange(): return lax.all_to_all(pieces, axes, 0, 0, tiled=True)]
    pallas_call x1, Pallas kernels: 2.68 us -> 0.86 us  [span_terms(): pl.pallas_call(span_kernel, in_specs=[pl.BlockSpec(memory_space=pltpu.SME...]
    pallas_call x1 -> x2, Pallas kernels: 3.67 us -> 2.63 us  [the longest x1 1.35 us: hidden_terms(): pl.pallas_call(hidden_kernel, in_specs=[VMEM] * 4 + [pl.BlockSpec(memory_...]
  transfers between devices with their start and end apart: 5 -> 4, of which waited for: 2 -> 1; matrix products, arithmetic and copies ran while one was open for 0% -> 1% of each run, Pallas kernels for 2% -> 0%
where the time goes in v3:
time: 173 us; the launch traced here: 172 us
  blocking collectives  106 us (61%)
  starting transfers between devices  51.9 us (30%)
  Pallas kernels  5.63 us (3%)
  local copies, waits for them, and re-layouts  2.81 us (2%)
  waiting for transfers between devices  2.23 us (1%)
  matrix products  1.75 us (1%)
    all_to_all x6, blocking collectives, exchange(): return lax.all_to_all(pieces, axes, 0, 0, tiled=True)  106 us
    all_to_all x1, starting transfers between devices, exchange(): return lax.all_to_all(pieces, axes, 0, 0, tiled=True)  44.4 us
  transfers between devices with their start and end apart: 4, of which 1 were waited for; matrix products, arithmetic and copies ran while one was open for 1% of the time, Pallas kernels for 0%

profile of v3, /device:TPU:65, one launch (start us, length us, event | category | flops | bytes accessed | tf_op | source)
XLA Modules:
  0.0 172.3 jit_solution(11831877121485893650)
XLA Ops:
  0.0 2.1 %project.1 = bf16[128,1024]{1,0:T(8,128)(2,1)} custom-call(bf16[128,256]{1,0:T(8,128)(2,1)} %tokens.1, f32[1,256]{1,0:T(1,128)} %bitcast.25, bf16[256,128]{1,0:T(8,128)(2,1)} %refs_0_.1, bf16[256,128]{1,0:T(8,128)(2,1)} %refs_1_.1, bf16[256,128]{1,0:T(8,128)(2,1)} %refs_2_.1, bf16[256,256]{1,0:T(8,128)(2,1)} %refs_3_.1, bf16[256,256]{1,0:T(8,128)(2,1)} %refs_4_.1), custom_call_target="tpu_custom_call" | custom-call | tf_op jit(solution)/shard_map/project/pallas_call | solution.py:60
  2.1 44.4 %all-to-all-start = ((bf16[16,8,1024]{2,1,0:T(8,128)(2,1)}), bf16[16,8,1024]{2,1,0:T(8,128)(2,1)S(1)}, u32[]{:S(2)}, u32[]{:S(2)}) async-start(bf16[16,8,1024]{2,1,0:T(8,128)(2,1)} %bitcast.22), calls=%async_computation | async-start | bytes 524288 | tf_op jit(solution)/shard_map/all_to_all | solution.py:22
  46.5 3.1 %collective-permute-start.1 = (bf16[256,1024]{1,0:T(8,128)(2,1)}, bf16[256,1024]{1,0:T(8,128)(2,1)}, u32[]{:S(2)}, u32[]{:S(2)}) collective-permute-start(bf16[256,1024]{1,0:T(8,128)(2,1)} %first.1), channel_id=1, source_target_pairs={{0,1},{1,0},{2,3},{3,2},{4,5},{5,4},{6,7},{7,6},{8,9},{9,8},{10,11... | collective-permute-start | bytes 1572872 | tf_op jit(solution)/shard_map/ppermute | solution.py:273
  49.6 2.0 %collective-permute-start.2 = (bf16[1024,256]{1,0:T(8,128)(2,1)}, bf16[1024,256]{1,0:T(8,128)(2,1)}, u32[]{:S(2)}, u32[]{:S(2)}) collective-permute-start(bf16[1024,256]{1,0:T(8,128)(2,1)} %param.35), channel_id=1, source_target_pairs={{0,1},{1,0},{2,3},{3,2},{4,5},{5,4},{6,7},{7,6},{8,9},{9,8},{10,11... | collective-permute-start | bytes 1572872 | tf_op jit(solution)/shard_map/ppermute | solution.py:274
  51.6 2.4 %collective-permute-start = (bf16[256,256]{1,0:T(8,128)(2,1)}, bf16[256,256]{1,0:T(8,128)(2,1)}, u32[]{:S(2)}, u32[]{:S(2)}) collective-permute-start(bf16[256,256]{1,0:T(8,128)(2,1)} %param.32), channel_id=1, source_target_pairs={{0,1},{1,0},{2,3},{3,2},{4,5},{5,4},{6,7},{7,6},{8,9},{9,8},{10,11... | collective-permute-start | bytes 393224 | tf_op jit(solution)/shard_map/ppermute | solution.py:272
  54.1 0.0 copy-start.8
  54.2 0.6 copy-done.7
  54.8 0.0 copy-done.8
  54.8 0.1 copy-done.5
  54.9 1.0 copy-done.2
  55.9 0.9 span.1
  56.8 1.0 broadcast_select_fusion
  57.8 2.2 %all-to-all-done.arrived = bf16[16,8,1024]{2,1,0:T(8,128)(2,1)S(1)} async-done(((bf16[16,8,1024]{2,1,0:T(8,128)(2,1)}), bf16[16,8,1024]{2,1,0:T(8,128)(2,1)S(1)}, u32[]{:S(2)}, u32[]{:S(2)}) %all-to-all-start) | async-done | bytes 262176 | tf_op jit(solution)/shard_map/all_to_all | solution.py:22
  60.1 1.3 attend.1
  61.4 24.2 %all_to_all.35 = bf16[32,4,256]{2,1,0:T(4,128)(2,1)S(1)} all-to-all(bf16[32,4,256]{2,1,0:T(4,128)(2,1)S(1)} %attend.1), channel_id=1, replica_groups=mesh['grp'=2,'kv'=16,'x'=8,'core'=2] {'kv','core'}, dimensions={0} | all-to-all | bytes 131072 | tf_op jit(solution)/shard_map/all_to_all | solution.py:22
  85.6 0.1 fusion.13
  85.8 0.2 fusion
  86.0 16.1 %all_to_all.36.arrived = bf16[8,64,256]{2,1,0:T(8,128)(2,1)S(1)} all-to-all(bf16[8,64,256]{2,1,0:T(8,128)(2,1)S(1)} %broadcast_in_dim.8), channel_id=1, replica_groups=mesh['grp'=2,'kv'=16,'x'=8,'core'=2] {'x'}, dimensions={0} | all-to-all | bytes 524288 | tf_op jit(solution)/shard_map/all_to_all | solution.py:22
  102.1 1.3 hidden.1
  103.5 18.9 %all_to_all.37 = bf16[16,4,2176]{2,1,0:T(4,128)(2,1)S(1)} all-to-all(bf16[16,4,2176]{2,1,0:T(4,128)(2,1)S(1)} %get-tuple-element.39), channel_id=1, replica_groups=mesh['grp'=2,'kv'=16,'x'=8,'core'=2] {'kv'}, dimensions={0} | all-to-all | bytes 557056 | tf_op jit(solution)/shard_map/all_to_all | solution.py:22
  122.4 0.1 convert_reduce_fusion
  122.5 0.2 fusion.11
  122.7 0.1 fusion.7
  122.8 0.1 broadcast_in_dim.9
  122.9 24.9 %all_to_all.38 = bf16[16,4,2048]{2,1,0:T(4,128)(2,1)S(1)} all-to-all(bf16[16,4,2048]{2,1,0:T(4,128)(2,1)S(1)} %broadcast_in_dim.9), channel_id=1, replica_groups=mesh['grp'=2,'kv'=16,'x'=8,'core'=2] {'kv'}, dimensions={0} | all-to-all | bytes 524288 | tf_op jit(solution)/shard_map/all_to_all | solution.py:22
  147.8 0.1 reshape.46
  147.9 0.2 fusion.3
  148.1 1.2 fusion.1
  149.4 11.8 %all_to_all.39 = bf16[8,64,256]{2,1,0:T(8,128)(2,1)S(1)} all-to-all(bf16[8,64,256]{2,1,0:T(8,128)(2,1)S(1)} %broadcast_in_dim.10), channel_id=1, replica_groups=mesh['grp'=2,'kv'=16,'x'=8,'core'=2] {'x'}, dimensions={0} | all-to-all | bytes 524288 | tf_op jit(solution)/shard_map/all_to_all | solution.py:22
  161.2 10.3 %all_to_all.40 = bf16[2,64,256]{2,1,0:T(8,128)(2,1)S(1)} all-to-all(bf16[2,64,256]{2,1,0:T(8,128)(2,1)S(1)} %broadcast_in_dim.11), channel_id=1, replica_groups=mesh['grp'=2,'kv'=16,'x'=8,'core'=2] {'core'}, dimensions={0} | all-to-all | bytes 131072 | tf_op jit(solution)/shard_map/all_to_all | solution.py:22
  171.6 0.1 copy.33
  171.7 0.7 reshape.48
  (32 shorter events, 0.3 us)
Async XLA Ops:
  0.0 54.2 %copy-start.1 = (f32[8,128,256]{2,1,0:T(8,128)S(1)}, f32[8,128,256]{2,1,0:T(8,128)}, u32[]{:S(2)}) copy-start(f32[8,128,256]{2,1,0:T(8,128)} %decays.1) | copy-start | bytes 3145732
  2.1 51.9 %copy-start.10 = (bf16[128,256]{1,0:T(8,128)(2,1)S(1)}, bf16[128,256]{1,0:T(8,128)(2,1)}, u32[]{:S(2)}) copy-start(bf16[128,256]{1,0:T(8,128)(2,1)} %tokens.1) | copy-start | bytes 196612
  2.1 57.9 %all-to-all-start = ((bf16[16,8,1024]{2,1,0:T(8,128)(2,1)}), bf16[16,8,1024]{2,1,0:T(8,128)(2,1)S(1)}, u32[]{:S(2)}, u32[]{:S(2)}) async-start(bf16[16,8,1024]{2,1,0:T(8,128)(2,1)} %bitcast.22), calls=%async_computation | async-start | bytes 524288 | tf_op jit(solution)/shard_map/all_to_all | solution.py:22
  46.5 11.3 %collective-permute-start.1 = (bf16[256,1024]{1,0:T(8,128)(2,1)}, bf16[256,1024]{1,0:T(8,128)(2,1)}, u32[]{:S(2)}, u32[]{:S(2)}) collective-permute-start(bf16[256,1024]{1,0:T(8,128)(2,1)} %first.1), channel_id=1, source_target_pairs={{0,1},{1,0},{2,3},{3,2},{4,5},{5,4},{6,7},{7,6},{8,9},{9,8},{10,11... | collective-permute-start | bytes 1572872 | tf_op jit(solution)/shard_map/ppermute | solution.py:273
  49.6 8.2 %collective-permute-start.2 = (bf16[1024,256]{1,0:T(8,128)(2,1)}, bf16[1024,256]{1,0:T(8,128)(2,1)}, u32[]{:S(2)}, u32[]{:S(2)}) collective-permute-start(bf16[1024,256]{1,0:T(8,128)(2,1)} %param.35), channel_id=1, source_target_pairs={{0,1},{1,0},{2,3},{3,2},{4,5},{5,4},{6,7},{7,6},{8,9},{9,8},{10,11... | collective-permute-start | bytes 1572872 | tf_op jit(solution)/shard_map/ppermute | solution.py:274
  51.6 5.2 %collective-permute-start = (bf16[256,256]{1,0:T(8,128)(2,1)}, bf16[256,256]{1,0:T(8,128)(2,1)}, u32[]{:S(2)}, u32[]{:S(2)}) collective-permute-start(bf16[256,256]{1,0:T(8,128)(2,1)} %param.32), channel_id=1, source_target_pairs={{0,1},{1,0},{2,3},{3,2},{4,5},{5,4},{6,7},{7,6},{8,9},{9,8},{10,11... | collective-permute-start | bytes 393224 | tf_op jit(solution)/shard_map/ppermute | solution.py:272
  54.1 0.7 copy-start.7
  54.1 0.7 copy-start.8
  54.2 0.7 copy-start.5
  54.2 0.7 copy-start.6
  54.8 1.0 copy-start.2
  55.9 4.2 %copy-start = (bf16[8,256,256]{2,1,0:T(8,128)(2,1)S(1)}, bf16[8,256,256]{2,1,0:T(8,128)(2,1)}, u32[]{:S(2)}) copy-start(bf16[8,256,256]{2,1,0:T(8,128)(2,1)} %values.1) | copy-start | bytes 3145732
  56.8 3.3 %copy-start.4 = (f32[8,4,32,64]{3,2,1,0:T(8,128)S(1)}, f32[8,4,32,64]{3,2,1,0:T(8,128)}, u32[]{:S(2)}) copy-start(f32[8,4,32,64]{3,2,1,0:T(8,128)} %state.1) | copy-start | bytes 786436
  85.8 16.3 %copy-start.3 = (bf16[256,1024]{1,0:T(8,128)(2,1)S(1)}, bf16[256,1024]{1,0:T(8,128)(2,1)}, u32[]{:S(2)}) copy-start(bf16[256,1024]{1,0:T(8,128)(2,1)} %first.1) | copy-start | bytes 1572868
  122.9 25.0 %copy-start.9 = (bf16[1024,256]{1,0:T(8,128)(2,1)S(1)}, bf16[1024,256]{1,0:T(8,128)(2,1)}, u32[]{:S(2)}) copy-start(bf16[1024,256]{1,0:T(8,128)(2,1)} %param.35) | copy-start | bytes 1572868

commit v4 on v3

--- a/solution.py
+++ b/solution.py
@@ -32,6 +32,7 @@
 
 
 VMEM = pl.BlockSpec(memory_space=pltpu.VMEM)
+ANY = pl.BlockSpec(memory_space=pl.ANY)
 
 
 def dot(a, b):
@@ -105,7 +106,14 @@
     )(lengths, keys, decays, *(v.reshape(1, -1) for v in (head_gain, bias, wide_gain)))
 
 
-def attend_kernel(arrived, weighted, start_factor, bias, gain, values, state, out):
+def attend_kernel(arrived, weighted, start_factor, bias, gain, values, state, *refs):
+    count = len(refs) // 2 - 1
+    far, (out, *near, done) = refs[:count], refs[count:]
+    copies = [
+        pltpu.make_async_copy(a, b, done.at[i]) for i, (a, b) in enumerate(zip(far, near))
+    ]
+    for copy in copies:
+        copy.start()
     seq_count, channels = start_factor.shape
     heads = channels // KEY_WIDTH
     width = heads * DV
@@ -177,24 +185,35 @@
         piece = low[c * half : (c + 1) * half]
         for k in range(out.shape[0] // CORES):
             out[k * CORES + c] = piece
-
-
-def attend(arrived, weighted, start_factor, values, state, bias, gain):
+    for copy in copies:
+        copy.wait()
+
+
+def attend(arrived, weighted, start_factor, values, state, bias, gain, shards_far):
     seq_count, width = values.shape[:2]
     half = seq_count // CORES
+    count = len(shards_far)
     return pl.pallas_call(
         attend_kernel,
-        in_specs=[VMEM] * 7,
-        out_specs=VMEM,
-        out_shape=pltpu.VMEM((arrived.shape[0] * CORES, half, width), bf16),
+        in_specs=[VMEM] * 7 + [ANY] * count,
+        out_specs=(VMEM,) * (1 + count),
+        out_shape=(
+            pltpu.VMEM((arrived.shape[0] * CORES, half, width), bf16),
+            *(pltpu.VMEM(v.shape, v.dtype) for v in shards_far),
+        ),
+        scratch_shapes=[pltpu.SemaphoreType.DMA((count,))],
         compiler_params=pltpu.CompilerParams(vmem_limit_bytes=16 << 20),
         name="attend",
-    )(*in_vmem(arrived, weighted, start_factor, bias, gain, values, state))
-
-
-def hidden_kernel(arrived, tokens, gain, first, second_far, out, resid, second, done):
-    copy = pltpu.make_async_copy(second_far, second, done)
-    copy.start()
+    )(*in_vmem(arrived, weighted, start_factor, bias, gain, values, state), *shards_far)
+
+
+def hidden_kernel(
+    arrived, tokens, gain, first, second_far, shard_far, out, resid, shard, second, done
+):
+    second_copy = pltpu.make_async_copy(second_far, second, done.at[0])
+    second_copy.start()
+    shard_copy = pltpu.make_async_copy(shard_far, shard, done.at[1])
+    shard_copy.start()
     total = arrived[0].astype(f32)
     for x in range(1, arrived.shape[0]):
         total += arrived[x].astype(f32)
@@ -216,24 +235,54 @@
 
     put(0, dot(scaled, first[...]).astype(bf16))
     put(2 * own, squares)
-    copy.wait()
+    second_copy.wait()
     put(own, dot(scaled, second[...]).astype(bf16))
-
-
-def hidden_terms(arrived, tokens, gain, first, second, peers):
+    shard_copy.wait()
+
+
+def hidden_terms(arrived, tokens, gain, first, second, shard, peers):
     rows, width = tokens.shape
     return pl.pallas_call(
         hidden_kernel,
-        in_specs=[VMEM] * 4 + [pl.BlockSpec(memory_space=pl.ANY)],
-        out_specs=(VMEM, VMEM),
+        in_specs=[VMEM] * 4 + [ANY] * 2,
+        out_specs=(VMEM,) * 3,
         out_shape=(
             pltpu.VMEM((peers, rows // peers, 2 * first.shape[1] + LANES), bf16),
             pltpu.VMEM((rows, width), bf16),
+            pltpu.VMEM(shard.shape, shard.dtype),
         ),
-        scratch_shapes=[pltpu.VMEM(second.shape, second.dtype), pltpu.SemaphoreType.DMA(())],
+        scratch_shapes=[
+            pltpu.VMEM(second.shape, second.dtype),
+            pltpu.SemaphoreType.DMA((2,)),
+        ],
         compiler_params=pltpu.CompilerParams(vmem_limit_bytes=16 << 20),
         name="hidden",
-    )(*in_vmem(arrived, tokens, gain, first), second)
+    )(*in_vmem(arrived, tokens, gain, first), second, shard)
+
+
+def active_kernel(arrived, out):
+    count = out.shape[2]
+    total = arrived[0].astype(f32)
+    for k in range(1, arrived.shape[0]):
+        total += arrived[k].astype(f32)
+    square = jnp.sum(total[:, count:], axis=1, keepdims=True)
+    before = total[:, :count] * lax.rsqrt(square / D + NORM_EPS)
+    up = jnp.maximum(before, 0.0)
+    low = (up * up).astype(bf16)
+    for k in range(out.shape[0]):
+        out[k] = low
+
+
+def active(arrived):
+    pieces, rows, width = arrived.shape
+    return pl.pallas_call(
+        active_kernel,
+        in_specs=[VMEM],
+        out_specs=VMEM,
+        out_shape=pltpu.VMEM((pieces, rows, width - LANES), bf16),
+        compiler_params=pltpu.CompilerParams(vmem_limit_bytes=8 << 20),
+        name="active",
+    )(*in_vmem(arrived))
 
 
 def shards(
@@ -287,27 +336,34 @@
     )
     weighted, start_factor, gain, bias, wide_gain = ready
 
-    spread = attend(arrived, weighted, start_factor, value_cache, block_state, bias, gain)
+    spread, out_first, out_second = attend(
+        arrived,
+        weighted,
+        start_factor,
+        value_cache,
+        block_state,
+        bias,
+        gain,
+        (out_first, out_second),
+    )
     heads = exchange(spread, ("kv", "core")).reshape(peers, CORES, half, values)
     attn_terms = dot(heads[:, 0].reshape(rows_half, values), out_first) + dot(
         heads[:, 1].reshape(rows_half, values), out_second
     )
     attn_arrived = to_everyone(attn_terms.astype(bf16), "x")
-    up_sent, resid = hidden_terms(
-        attn_arrived, own_tokens, wide_gain, up_weight, up_other, peers
-    )
-    up_total = jnp.sum(exchange(up_sent, "kv").astype(f32), axis=0)
-    hidden_count = up_weight.shape[1] * CORES
-    before, squares = up_total[:, :hidden_count], up_total[:, hidden_count:]
-    mixer_scale = lax.rsqrt((squares[:, :1] + squares[:, 1:2]) / D + NORM_EPS)
-    hidden = jnp.square(jax.nn.relu(before * mixer_scale)).astype(bf16)
-    every = to_everyone(hidden, "kv").reshape(rows_half, hidden_count)
+    up_sent, resid, down_other = hidden_terms(
+        attn_arrived, own_tokens, wide_gain, up_weight, up_other, down_other, peers
+    )
+    hidden = active(exchange(up_sent, "kv"))
+    every = exchange(hidden, "kv").reshape(rows_half, -1)
     own_count = up_weight.shape[1]
     down_terms = dot(every[:, :own_count], down_weight) + dot(every[:, own_count:], down_other)
     mixer_out = jnp.sum(to_everyone(down_terms.astype(bf16), "x").astype(f32), axis=0)
     own_out = (resid.astype(f32) + mixer_out).astype(bf16)
-    both = to_everyone(own_out, "core").reshape(CORES, peers, half, -1)
-    return jnp.swapaxes(both, 0, 1).reshape(peers * seq_count, -1)
+    other_out = lax.ppermute(own_out, "core", swap)
+    low_half = jnp.where(core == 0, own_out, other_out).reshape(peers, half, -1)
+    high_half = jnp.where(core == 0, other_out, own_out).reshape(peers, half, -1)
+    return jnp.concatenate([low_half, high_half], axis=1).reshape(peers * seq_count, -1)
 
 
 def solution(mesh):

time: 173 us -> 171 us (0.988)
  blocking collectives: 106 us -> 95.9 us
  starting transfers between devices: 51.9 us -> 60.7 us
    all_to_all x6 -> x5, blocking collectives: 106 us -> 95.9 us  [exchange(): return lax.all_to_all(pieces, axes, 0, 0, tiled=True)]
    ppermute x0 -> x1, starting transfers between devices: none -> 8.83 us  [shards(): other_out = lax.ppermute(own_out, 'core', swap)]
  transfers between devices with their start and end apart: 4 -> 5, of which waited for: 1 -> 2; matrix products, arithmetic and copies ran while one was open for 1% -> 1% of each run, Pallas kernels for 0% -> 1%
where the time goes in v4:
time: 171 us
  blocking collectives  95.9 us (56%)
  starting transfers between devices  60.7 us (35%)
  Pallas kernels  6.13 us (4%)
  waiting for transfers between devices  3.06 us (2%)
  local copies, waits for them, and re-layouts  2 us (1%)
  other arithmetic  1.77 us (1%)
    all_to_all x5, blocking collectives, exchange(): return lax.all_to_all(pieces, axes, 0, 0, tiled=True)  95.9 us
    all_to_all x1, starting transfers between devices, exchange(): return lax.all_to_all(pieces, axes, 0, 0, tiled=True)  44.4 us
    ppermute x1, starting transfers between devices, shards(): other_out = lax.ppermute(own_out, 'core', swap)  8.83 us
  transfers between devices with their start and end apart: 5, of which 2 were waited for; matrix products, arithmetic and copies ran while one was open for 1% of the time, Pallas kernels for 1%

profile of v4, /device:TPU:65, one launch (start us, length us, event | category | flops | bytes accessed | tf_op | source)
XLA Modules:
  0.0 170.6 jit_solution(1132529856865149186)
XLA Ops:
  0.0 2.2 %project.1 = bf16[128,1024]{1,0:T(8,128)(2,1)} custom-call(bf16[128,256]{1,0:T(8,128)(2,1)} %tokens.1, f32[1,256]{1,0:T(1,128)} %bitcast.23, bf16[256,128]{1,0:T(8,128)(2,1)} %refs_0_.1, bf16[256,128]{1,0:T(8,128)(2,1)} %refs_1_.1, bf16[256,128]{1,0:T(8,128)(2,1)} %refs_2_.1, bf16[256,256]{1,0:T(8,128)(2,1)} %refs_3_.1, bf16[256,256]{1,0:T(8,128)(2,1)} %refs_4_.1), custom_call_target="tpu_custom_call" | custom-call | tf_op jit(solution)/shard_map/project/pallas_call | solution.py:61
  2.2 44.4 %all-to-all-start = ((bf16[16,8,1024]{2,1,0:T(8,128)(2,1)}), bf16[16,8,1024]{2,1,0:T(8,128)(2,1)S(1)}, u32[]{:S(2)}, u32[]{:S(2)}) async-start(bf16[16,8,1024]{2,1,0:T(8,128)(2,1)} %bitcast.21), calls=%async_computation | async-start | bytes 524288 | tf_op jit(solution)/shard_map/all_to_all | solution.py:22
  46.5 3.1 %collective-permute-start.1 = (bf16[256,1024]{1,0:T(8,128)(2,1)}, bf16[256,1024]{1,0:T(8,128)(2,1)}, u32[]{:S(2)}, u32[]{:S(2)}) collective-permute-start(bf16[256,1024]{1,0:T(8,128)(2,1)} %first.1), channel_id=1, source_target_pairs={{0,1},{1,0},{2,3},{3,2},{4,5},{5,4},{6,7},{7,6},{8,9},{9,8},{10,11... | collective-permute-start | bytes 1572872 | tf_op jit(solution)/shard_map/ppermute | solution.py:322
  49.6 2.0 %collective-permute-start.2 = (bf16[1024,256]{1,0:T(8,128)(2,1)}, bf16[1024,256]{1,0:T(8,128)(2,1)}, u32[]{:S(2)}, u32[]{:S(2)}) collective-permute-start(bf16[1024,256]{1,0:T(8,128)(2,1)} %param.35), channel_id=1, source_target_pairs={{0,1},{1,0},{2,3},{3,2},{4,5},{5,4},{6,7},{7,6},{8,9},{9,8},{10,11... | collective-permute-start | bytes 1572872 | tf_op jit(solution)/shard_map/ppermute | solution.py:323
  51.6 2.4 %collective-permute-start = (bf16[256,256]{1,0:T(8,128)(2,1)}, bf16[256,256]{1,0:T(8,128)(2,1)}, u32[]{:S(2)}, u32[]{:S(2)}) collective-permute-start(bf16[256,256]{1,0:T(8,128)(2,1)} %param.32), channel_id=1, source_target_pairs={{0,1},{1,0},{2,3},{3,2},{4,5},{5,4},{6,7},{7,6},{8,9},{9,8},{10,11... | collective-permute-start | bytes 393224 | tf_op jit(solution)/shard_map/ppermute | solution.py:321
  54.1 0.0 copy-start.7
  54.2 0.0 copy-start.5
  54.2 0.0 copy-start.6
  54.2 0.6 copy-done.7
  54.8 0.0 copy-done.8
  54.8 0.1 copy-done.5
  54.9 1.0 copy-done.2
  55.9 0.9 span.1
  56.8 0.0 copy-start.3
  56.8 1.0 broadcast_select_fusion
  57.9 2.2 %all-to-all-done.arrived = bf16[16,8,1024]{2,1,0:T(8,128)(2,1)S(1)} async-done(((bf16[16,8,1024]{2,1,0:T(8,128)(2,1)}), bf16[16,8,1024]{2,1,0:T(8,128)(2,1)S(1)}, u32[]{:S(2)}, u32[]{:S(2)}) %all-to-all-start) | async-done | bytes 262176 | tf_op jit(solution)/shard_map/all_to_all | solution.py:22
  60.1 1.6 attend.1
  61.7 24.2 %all_to_all.30 = bf16[32,4,256]{2,1,0:T(4,128)(2,1)S(1)} all-to-all(bf16[32,4,256]{2,1,0:T(4,128)(2,1)S(1)} %get-tuple-element.39), channel_id=1, replica_groups=mesh['grp'=2,'kv'=16,'x'=8,'core'=2] {'kv','core'}, dimensions={0} | all-to-all | bytes 131072 | tf_op jit(solution)/shard_map/all_to_all | solution.py:22
  86.0 0.1 fusion.6
  86.1 0.2 fusion
  86.3 16.1 %all_to_all.31.arrived = bf16[8,64,256]{2,1,0:T(8,128)(2,1)S(1)} all-to-all(bf16[8,64,256]{2,1,0:T(8,128)(2,1)S(1)} %broadcast_in_dim.4), channel_id=1, replica_groups=mesh['grp'=2,'kv'=16,'x'=8,'core'=2] {'x'}, dimensions={0} | all-to-all | bytes 524288 | tf_op jit(solution)/shard_map/all_to_all | solution.py:22
  102.5 1.4 hidden.1
  103.8 18.9 %all_to_all.32.arrived = bf16[16,4,2176]{2,1,0:T(4,128)(2,1)S(1)} all-to-all(bf16[16,4,2176]{2,1,0:T(4,128)(2,1)S(1)} %get-tuple-element.47), channel_id=1, replica_groups=mesh['grp'=2,'kv'=16,'x'=8,'core'=2] {'kv'}, dimensions={0} | all-to-all | bytes 557056 | tf_op jit(solution)/shard_map/all_to_all | solution.py:22
  122.7 0.1 active.1
  122.9 24.9 %all_to_all.33 = bf16[16,4,2048]{2,1,0:T(4,128)(2,1)S(1)} all-to-all(bf16[16,4,2048]{2,1,0:T(4,128)(2,1)S(1)} %active.1), channel_id=1, replica_groups=mesh['grp'=2,'kv'=16,'x'=8,'core'=2] {'kv'}, dimensions={0} | all-to-all | bytes 524288 | tf_op jit(solution)/shard_map/all_to_all | solution.py:22
  147.8 0.1 reshape.47
  147.9 0.2 fusion.3
  148.1 0.2 fusion.1
  148.3 11.8 %all_to_all.34 = bf16[8,64,256]{2,1,0:T(8,128)(2,1)S(1)} all-to-all(bf16[8,64,256]{2,1,0:T(8,128)(2,1)S(1)} %broadcast_in_dim.5), channel_id=1, replica_groups=mesh['grp'=2,'kv'=16,'x'=8,'core'=2] {'x'}, dimensions={0} | all-to-all | bytes 524288 | tf_op jit(solution)/shard_map/all_to_all | solution.py:22
  160.2 8.8 %collective-permute-start.3 = (bf16[64,256]{1,0:T(8,128)(2,1)S(1)}, bf16[64,256]{1,0:T(8,128)(2,1)S(1)}, u32[]{:S(2)}, u32[]{:S(2)}) collective-permute-start(bf16[64,256]{1,0:T(8,128)(2,1)S(1)} %add_convert_fusion), channel_id=1, source_target_pairs={{0,1},{1,0},{2,3},{3,2},{4,5},{5,4},{6,7},{7,6},{8,9},{9,8},{10,11... | collective-permute-start | bytes 98312 | tf_op jit(solution)/shard_map/ppermute | solution.py:363
  169.0 0.8 collective-permute-done.3
  169.9 0.7 maximum_bitcast_fusion
  (30 shorter events, 0.3 us)
Async XLA Ops:
  0.0 54.2 %copy-start.1 = (f32[8,128,256]{2,1,0:T(8,128)S(1)}, f32[8,128,256]{2,1,0:T(8,128)}, u32[]{:S(2)}) copy-start(f32[8,128,256]{2,1,0:T(8,128)} %decays.1) | copy-start | bytes 3145732
  2.2 51.9 %copy-start.10 = (bf16[128,256]{1,0:T(8,128)(2,1)S(1)}, bf16[128,256]{1,0:T(8,128)(2,1)}, u32[]{:S(2)}) copy-start(bf16[128,256]{1,0:T(8,128)(2,1)} %tokens.1) | copy-start | bytes 196612
  2.2 57.9 %all-to-all-start = ((bf16[16,8,1024]{2,1,0:T(8,128)(2,1)}), bf16[16,8,1024]{2,1,0:T(8,128)(2,1)S(1)}, u32[]{:S(2)}, u32[]{:S(2)}) async-start(bf16[16,8,1024]{2,1,0:T(8,128)(2,1)} %bitcast.21), calls=%async_computation | async-start | bytes 524288 | tf_op jit(solution)/shard_map/all_to_all | solution.py:22
  46.5 11.3 %collective-permute-start.1 = (bf16[256,1024]{1,0:T(8,128)(2,1)}, bf16[256,1024]{1,0:T(8,128)(2,1)}, u32[]{:S(2)}, u32[]{:S(2)}) collective-permute-start(bf16[256,1024]{1,0:T(8,128)(2,1)} %first.1), channel_id=1, source_target_pairs={{0,1},{1,0},{2,3},{3,2},{4,5},{5,4},{6,7},{7,6},{8,9},{9,8},{10,11... | collective-permute-start | bytes 1572872 | tf_op jit(solution)/shard_map/ppermute | solution.py:322
  49.6 8.2 %collective-permute-start.2 = (bf16[1024,256]{1,0:T(8,128)(2,1)}, bf16[1024,256]{1,0:T(8,128)(2,1)}, u32[]{:S(2)}, u32[]{:S(2)}) collective-permute-start(bf16[1024,256]{1,0:T(8,128)(2,1)} %param.35), channel_id=1, source_target_pairs={{0,1},{1,0},{2,3},{3,2},{4,5},{5,4},{6,7},{7,6},{8,9},{9,8},{10,11... | collective-permute-start | bytes 1572872 | tf_op jit(solution)/shard_map/ppermute | solution.py:323
  51.6 5.2 %collective-permute-start = (bf16[256,256]{1,0:T(8,128)(2,1)}, bf16[256,256]{1,0:T(8,128)(2,1)}, u32[]{:S(2)}, u32[]{:S(2)}) collective-permute-start(bf16[256,256]{1,0:T(8,128)(2,1)} %param.32), channel_id=1, source_target_pairs={{0,1},{1,0},{2,3},{3,2},{4,5},{5,4},{6,7},{7,6},{8,9},{9,8},{10,11... | collective-permute-start | bytes 393224 | tf_op jit(solution)/shard_map/ppermute | solution.py:321
  54.1 0.7 copy-start.7
  54.1 0.7 copy-start.8
  54.2 0.7 copy-start.5
  54.2 0.7 copy-start.6
  54.9 1.0 copy-start.2
  55.9 4.2 %copy-start = (bf16[8,256,256]{2,1,0:T(8,128)(2,1)S(1)}, bf16[8,256,256]{2,1,0:T(8,128)(2,1)}, u32[]{:S(2)}) copy-start(bf16[8,256,256]{2,1,0:T(8,128)(2,1)} %values.1) | copy-start | bytes 3145732
  56.8 3.3 %copy-start.3 = (f32[8,4,32,64]{3,2,1,0:T(8,128)S(1)}, f32[8,4,32,64]{3,2,1,0:T(8,128)}, u32[]{:S(2)}) copy-start(f32[8,4,32,64]{3,2,1,0:T(8,128)} %state.1) | copy-start | bytes 786436
  86.1 16.3 %copy-start.4 = (bf16[256,1024]{1,0:T(8,128)(2,1)S(1)}, bf16[256,1024]{1,0:T(8,128)(2,1)}, u32[]{:S(2)}) copy-start(bf16[256,1024]{1,0:T(8,128)(2,1)} %first.1) | copy-start | bytes 1572868
  122.9 25.0 %copy-start.9 = (bf16[1024,256]{1,0:T(8,128)(2,1)S(1)}, bf16[1024,256]{1,0:T(8,128)(2,1)}, u32[]{:S(2)}) copy-start(bf16[1024,256]{1,0:T(8,128)(2,1)} %param.35) | copy-start | bytes 1572868
  160.2 9.7 %collective-permute-start.3 = (bf16[64,256]{1,0:T(8,128)(2,1)S(1)}, bf16[64,256]{1,0:T(8,128)(2,1)S(1)}, u32[]{:S(2)}, u32[]{:S(2)}) collective-permute-start(bf16[64,256]{1,0:T(8,128)(2,1)S(1)} %add_convert_fusion), channel_id=1, source_target_pairs={{0,1},{1,0},{2,3},{3,2},{4,5},{5,4},{6,7},{7,6},{8,9},{9,8},{10,11... | collective-permute-start | bytes 98312 | tf_op jit(solution)/shard_map/ppermute | solution.py:363

commit v5 on v4

--- a/solution.py
+++ b/solution.py
@@ -11,6 +11,7 @@
 LANES = 128
 SUBLANES = 8
 CORES = 2
+STAGGER_NS = 4500
 
 NORM_EPS = 1e-06
 DECAY_SOFTNESS = 16.0
@@ -207,6 +208,29 @@
     )(*in_vmem(arrived, weighted, start_factor, bias, gain, values, state), *shards_far)
 
 
+def merge_kernel(heads_first, heads_second, first, second, out):
+    @pl.when(lax.axis_index("core") == 0)
+    def fall_behind():
+        pl.delay(STAGGER_NS)
+
+    terms = dot(heads_first[...], first[...]) + dot(heads_second[...], second[...])
+    low = terms.astype(bf16)
+    for x in range(out.shape[0]):
+        out[x] = low
+
+
+def merge(heads_first, heads_second, first, second, peers):
+    shape = (peers, heads_first.shape[0], first.shape[1])
+    return pl.pallas_call(
+        merge_kernel,
+        in_specs=[VMEM] * 4,
+        out_specs=VMEM,
+        out_shape=pltpu.VMEM(shape, bf16),
+        compiler_params=pltpu.CompilerParams(vmem_limit_bytes=8 << 20),
+        name="merge",
+    )(*in_vmem(heads_first, heads_second, first, second))
+
+
 def hidden_kernel(
     arrived, tokens, gain, first, second_far, shard_far, out, resid, shard, second, done
 ):
@@ -347,10 +371,14 @@
         (out_first, out_second),
     )
     heads = exchange(spread, ("kv", "core")).reshape(peers, CORES, half, values)
-    attn_terms = dot(heads[:, 0].reshape(rows_half, values), out_first) + dot(
-        heads[:, 1].reshape(rows_half, values), out_second
-    )
-    attn_arrived = to_everyone(attn_terms.astype(bf16), "x")
+    attn_terms = merge(
+        heads[:, 0].reshape(rows_half, values),
+        heads[:, 1].reshape(rows_half, values),
+        out_first,
+        out_second,
+        lax.axis_size("x"),
+    )
+    attn_arrived = exchange(attn_terms, "x")
     up_sent, resid, down_other = hidden_terms(
         attn_arrived, own_tokens, wide_gain, up_weight, up_other, down_other, peers
     )

time: 171 us -> 166 us (0.971)
  blocking collectives: 95.9 us -> 86.7 us
  starting transfers between devices: 60.7 us -> 64.6 us
    all_to_all x5, blocking collectives: 95.9 us -> 86.7 us  [exchange(): return lax.all_to_all(pieces, axes, 0, 0, tiled=True)]
    ppermute x1, starting transfers between devices: 8.83 us -> 12.8 us  [shards(): other_out = lax.ppermute(own_out, 'core', swap)]
where the time goes in v5:
time: 166 us; the launch traced here: 165 us
  blocking collectives  86.7 us (52%)
  starting transfers between devices  64.6 us (39%)
  Pallas kernels  6.31 us (4%)
  waiting for transfers between devices  3.07 us (2%)
  local copies, waits for them, and re-layouts  1.97 us (1%)
  other arithmetic  1.77 us (1%)
    all_to_all x5, blocking collectives, exchange(): return lax.all_to_all(pieces, axes, 0, 0, tiled=True)  86.7 us
    all_to_all x1, starting transfers between devices, exchange(): return lax.all_to_all(pieces, axes, 0, 0, tiled=True)  44.4 us
    ppermute x1, starting transfers between devices, shards(): other_out = lax.ppermute(own_out, 'core', swap)  12.8 us
  transfers between devices with their start and end apart: 5, of which 2 were waited for; matrix products, arithmetic and copies ran while one was open for 1% of the time, Pallas kernels for 1%

profile of v5, /device:TPU:65, one launch (start us, length us, event | category | flops | bytes accessed | tf_op | source)
XLA Modules:
  0.0 165.1 jit_solution(12011922475500723326)
XLA Ops:
  0.0 2.2 %project.1 = bf16[128,1024]{1,0:T(8,128)(2,1)} custom-call(bf16[128,256]{1,0:T(8,128)(2,1)} %tokens.1, f32[1,256]{1,0:T(1,128)} %bitcast.27, bf16[256,128]{1,0:T(8,128)(2,1)} %refs_0_.1, bf16[256,128]{1,0:T(8,128)(2,1)} %refs_1_.1, bf16[256,128]{1,0:T(8,128)(2,1)} %refs_2_.1, bf16[256,256]{1,0:T(8,128)(2,1)} %refs_3_.1, bf16[256,256]{1,0:T(8,128)(2,1)} %refs_4_.1), custom_call_target="tpu_custom_call" | custom-call | tf_op jit(solution)/shard_map/project/pallas_call | solution.py:62
  2.2 44.4 %all-to-all-start = ((bf16[16,8,1024]{2,1,0:T(8,128)(2,1)}), bf16[16,8,1024]{2,1,0:T(8,128)(2,1)S(1)}, u32[]{:S(2)}, u32[]{:S(2)}) async-start(bf16[16,8,1024]{2,1,0:T(8,128)(2,1)} %bitcast.25), calls=%async_computation | async-start | bytes 524288 | tf_op jit(solution)/shard_map/all_to_all | solution.py:23
  46.5 3.1 %collective-permute-start.1 = (bf16[256,1024]{1,0:T(8,128)(2,1)}, bf16[256,1024]{1,0:T(8,128)(2,1)}, u32[]{:S(2)}, u32[]{:S(2)}) collective-permute-start(bf16[256,1024]{1,0:T(8,128)(2,1)} %first.1), channel_id=1, source_target_pairs={{0,1},{1,0},{2,3},{3,2},{4,5},{5,4},{6,7},{7,6},{8,9},{9,8},{10,11... | collective-permute-start | bytes 1572872 | tf_op jit(solution)/shard_map/ppermute | solution.py:346
  49.6 2.0 %collective-permute-start.2 = (bf16[1024,256]{1,0:T(8,128)(2,1)}, bf16[1024,256]{1,0:T(8,128)(2,1)}, u32[]{:S(2)}, u32[]{:S(2)}) collective-permute-start(bf16[1024,256]{1,0:T(8,128)(2,1)} %param.35), channel_id=1, source_target_pairs={{0,1},{1,0},{2,3},{3,2},{4,5},{5,4},{6,7},{7,6},{8,9},{9,8},{10,11... | collective-permute-start | bytes 1572872 | tf_op jit(solution)/shard_map/ppermute | solution.py:347
  51.6 2.4 %collective-permute-start = (bf16[256,256]{1,0:T(8,128)(2,1)}, bf16[256,256]{1,0:T(8,128)(2,1)}, u32[]{:S(2)}, u32[]{:S(2)}) collective-permute-start(bf16[256,256]{1,0:T(8,128)(2,1)} %param.32), channel_id=1, source_target_pairs={{0,1},{1,0},{2,3},{3,2},{4,5},{5,4},{6,7},{7,6},{8,9},{9,8},{10,11... | collective-permute-start | bytes 393224 | tf_op jit(solution)/shard_map/ppermute | solution.py:345
  54.1 0.0 copy-start.7
  54.2 0.0 copy-start.5
  54.2 0.0 copy-start.6
  54.2 0.6 copy-done.7
  54.8 0.0 copy-done.8
  54.8 0.1 copy-done.5
  54.9 1.0 copy-done.2
  55.9 0.9 span.1
  56.8 0.0 copy-start.3
  56.8 1.0 broadcast_select_fusion
  57.9 2.2 %all-to-all-done.arrived = bf16[16,8,1024]{2,1,0:T(8,128)(2,1)S(1)} async-done(((bf16[16,8,1024]{2,1,0:T(8,128)(2,1)}), bf16[16,8,1024]{2,1,0:T(8,128)(2,1)S(1)}, u32[]{:S(2)}, u32[]{:S(2)}) %all-to-all-start) | async-done | bytes 262176 | tf_op jit(solution)/shard_map/all_to_all | solution.py:23
  60.1 1.6 attend.1
  61.7 24.2 %all_to_all.30 = bf16[32,4,256]{2,1,0:T(4,128)(2,1)S(1)} all-to-all(bf16[32,4,256]{2,1,0:T(4,128)(2,1)S(1)} %get-tuple-element.39), channel_id=1, replica_groups=mesh['grp'=2,'kv'=16,'x'=8,'core'=2] {'kv','core'}, dimensions={0} | all-to-all | bytes 131072 | tf_op jit(solution)/shard_map/all_to_all | solution.py:23
  86.0 0.0 copy-start.4
  86.0 0.2 merge.1
  86.2 16.2 %all_to_all.31.arrived = bf16[8,64,256]{2,1,0:T(8,128)(2,1)S(1)} all-to-all(bf16[8,64,256]{2,1,0:T(8,128)(2,1)S(1)} %merge.1), channel_id=1, replica_groups=mesh['grp'=2,'kv'=16,'x'=8,'core'=2] {'x'}, dimensions={0} | all-to-all | bytes 524288 | tf_op jit(solution)/shard_map/all_to_all | solution.py:23
  102.4 1.4 hidden.1
  103.7 15.7 %all_to_all.32.arrived = bf16[16,4,2176]{2,1,0:T(4,128)(2,1)S(1)} all-to-all(bf16[16,4,2176]{2,1,0:T(4,128)(2,1)S(1)} %get-tuple-element.47), channel_id=1, replica_groups=mesh['grp'=2,'kv'=16,'x'=8,'core'=2] {'kv'}, dimensions={0} | all-to-all | bytes 557056 | tf_op jit(solution)/shard_map/all_to_all | solution.py:23
  119.4 0.1 active.1
  119.5 18.9 %all_to_all.33 = bf16[16,4,2048]{2,1,0:T(4,128)(2,1)S(1)} all-to-all(bf16[16,4,2048]{2,1,0:T(4,128)(2,1)S(1)} %active.1), channel_id=1, replica_groups=mesh['grp'=2,'kv'=16,'x'=8,'core'=2] {'kv'}, dimensions={0} | all-to-all | bytes 524288 | tf_op jit(solution)/shard_map/all_to_all | solution.py:23
  138.4 0.1 reshape.46
  138.5 0.2 fusion.2
  138.7 0.2 fusion
  139.0 11.8 %all_to_all.34 = bf16[8,64,256]{2,1,0:T(8,128)(2,1)S(1)} all-to-all(bf16[8,64,256]{2,1,0:T(8,128)(2,1)S(1)} %broadcast_in_dim.2), channel_id=1, replica_groups=mesh['grp'=2,'kv'=16,'x'=8,'core'=2] {'x'}, dimensions={0} | all-to-all | bytes 524288 | tf_op jit(solution)/shard_map/all_to_all | solution.py:23
  150.8 12.8 %collective-permute-start.3 = (bf16[64,256]{1,0:T(8,128)(2,1)S(1)}, bf16[64,256]{1,0:T(8,128)(2,1)S(1)}, u32[]{:S(2)}, u32[]{:S(2)}) collective-permute-start(bf16[64,256]{1,0:T(8,128)(2,1)S(1)} %add_convert_fusion), channel_id=1, source_target_pairs={{0,1},{1,0},{2,3},{3,2},{4,5},{5,4},{6,7},{7,6},{8,9},{9,8},{10,11... | collective-permute-start | bytes 98312 | tf_op jit(solution)/shard_map/ppermute | solution.py:391
  163.6 0.8 collective-permute-done.3
  164.5 0.7 maximum_bitcast_fusion
  (28 shorter events, 0.3 us)
Async XLA Ops:
  0.0 54.2 %copy-start.1 = (f32[8,128,256]{2,1,0:T(8,128)S(1)}, f32[8,128,256]{2,1,0:T(8,128)}, u32[]{:S(2)}) copy-start(f32[8,128,256]{2,1,0:T(8,128)} %decays.1) | copy-start | bytes 3145732
  2.2 51.9 %copy-start.10 = (bf16[128,256]{1,0:T(8,128)(2,1)S(1)}, bf16[128,256]{1,0:T(8,128)(2,1)}, u32[]{:S(2)}) copy-start(bf16[128,256]{1,0:T(8,128)(2,1)} %tokens.1) | copy-start | bytes 196612
  2.2 57.9 %all-to-all-start = ((bf16[16,8,1024]{2,1,0:T(8,128)(2,1)}), bf16[16,8,1024]{2,1,0:T(8,128)(2,1)S(1)}, u32[]{:S(2)}, u32[]{:S(2)}) async-start(bf16[16,8,1024]{2,1,0:T(8,128)(2,1)} %bitcast.25), calls=%async_computation | async-start | bytes 524288 | tf_op jit(solution)/shard_map/all_to_all | solution.py:23
  46.5 11.3 %collective-permute-start.1 = (bf16[256,1024]{1,0:T(8,128)(2,1)}, bf16[256,1024]{1,0:T(8,128)(2,1)}, u32[]{:S(2)}, u32[]{:S(2)}) collective-permute-start(bf16[256,1024]{1,0:T(8,128)(2,1)} %first.1), channel_id=1, source_target_pairs={{0,1},{1,0},{2,3},{3,2},{4,5},{5,4},{6,7},{7,6},{8,9},{9,8},{10,11... | collective-permute-start | bytes 1572872 | tf_op jit(solution)/shard_map/ppermute | solution.py:346
  49.6 8.2 %collective-permute-start.2 = (bf16[1024,256]{1,0:T(8,128)(2,1)}, bf16[1024,256]{1,0:T(8,128)(2,1)}, u32[]{:S(2)}, u32[]{:S(2)}) collective-permute-start(bf16[1024,256]{1,0:T(8,128)(2,1)} %param.35), channel_id=1, source_target_pairs={{0,1},{1,0},{2,3},{3,2},{4,5},{5,4},{6,7},{7,6},{8,9},{9,8},{10,11... | collective-permute-start | bytes 1572872 | tf_op jit(solution)/shard_map/ppermute | solution.py:347
  51.6 5.2 %collective-permute-start = (bf16[256,256]{1,0:T(8,128)(2,1)}, bf16[256,256]{1,0:T(8,128)(2,1)}, u32[]{:S(2)}, u32[]{:S(2)}) collective-permute-start(bf16[256,256]{1,0:T(8,128)(2,1)} %param.32), channel_id=1, source_target_pairs={{0,1},{1,0},{2,3},{3,2},{4,5},{5,4},{6,7},{7,6},{8,9},{9,8},{10,11... | collective-permute-start | bytes 393224 | tf_op jit(solution)/shard_map/ppermute | solution.py:345
  54.1 0.7 copy-start.7
  54.1 0.7 copy-start.8
  54.2 0.7 copy-start.5
  54.2 0.7 copy-start.6
  54.9 1.0 copy-start.2
  55.9 4.2 %copy-start = (bf16[8,256,256]{2,1,0:T(8,128)(2,1)S(1)}, bf16[8,256,256]{2,1,0:T(8,128)(2,1)}, u32[]{:S(2)}) copy-start(bf16[8,256,256]{2,1,0:T(8,128)(2,1)} %values.1) | copy-start | bytes 3145732
  56.8 3.3 %copy-start.3 = (f32[8,4,32,64]{3,2,1,0:T(8,128)S(1)}, f32[8,4,32,64]{3,2,1,0:T(8,128)}, u32[]{:S(2)}) copy-start(f32[8,4,32,64]{3,2,1,0:T(8,128)} %state.1) | copy-start | bytes 786436
  86.0 16.4 %copy-start.4 = (bf16[256,1024]{1,0:T(8,128)(2,1)S(1)}, bf16[256,1024]{1,0:T(8,128)(2,1)}, u32[]{:S(2)}) copy-start(bf16[256,1024]{1,0:T(8,128)(2,1)} %first.1) | copy-start | bytes 1572868
  119.5 19.0 %copy-start.9 = (bf16[1024,256]{1,0:T(8,128)(2,1)S(1)}, bf16[1024,256]{1,0:T(8,128)(2,1)}, u32[]{:S(2)}) copy-start(bf16[1024,256]{1,0:T(8,128)(2,1)} %param.35) | copy-start | bytes 1572868
  150.8 13.6 %collective-permute-start.3 = (bf16[64,256]{1,0:T(8,128)(2,1)S(1)}, bf16[64,256]{1,0:T(8,128)(2,1)S(1)}, u32[]{:S(2)}, u32[]{:S(2)}) collective-permute-start(bf16[64,256]{1,0:T(8,128)(2,1)S(1)} %add_convert_fusion), channel_id=1, source_target_pairs={{0,1},{1,0},{2,3},{3,2},{4,5},{5,4},{6,7},{7,6},{8,9},{9,8},{10,11... | collective-permute-start | bytes 98312 | tf_op jit(solution)/shard_map/ppermute | solution.py:391

commit v6 on v5

--- a/solution.py
+++ b/solution.py
@@ -11,7 +11,7 @@
 LANES = 128
 SUBLANES = 8
 CORES = 2
-STAGGER_NS = 4500
+STAGGER_NS = 5600
 
 NORM_EPS = 1e-06
 DECAY_SOFTNESS = 16.0

time: 166 us -> 167 us (level)
  no operation moved by 1% of the time
where the time goes in v6:
time: 167 us; the launch traced here: 166 us
  blocking collectives  86.7 us (52%)
  starting transfers between devices  65.7 us (39%)
  Pallas kernels  6.31 us (4%)
  waiting for transfers between devices  3.07 us (2%)
  local copies, waits for them, and re-layouts  1.97 us (1%)
  other arithmetic  1.77 us (1%)
    all_to_all x5, blocking collectives, exchange(): return lax.all_to_all(pieces, axes, 0, 0, tiled=True)  86.7 us
    all_to_all x1, starting transfers between devices, exchange(): return lax.all_to_all(pieces, axes, 0, 0, tiled=True)  44.4 us
    ppermute x1, starting transfers between devices, shards(): other_out = lax.ppermute(own_out, 'core', swap)  13.8 us
  transfers between devices with their start and end apart: 5, of which 2 were waited for; matrix products, arithmetic and copies ran while one was open for 1% of the time, Pallas kernels for 1%

profile of v6, /device:TPU:65, one launch (start us, length us, event | category | flops | bytes accessed | tf_op | source)
XLA Modules:
  0.0 166.2 jit_solution(5518349094710227646)
XLA Ops:
  0.0 2.2 %project.1 = bf16[128,1024]{1,0:T(8,128)(2,1)} custom-call(bf16[128,256]{1,0:T(8,128)(2,1)} %tokens.1, f32[1,256]{1,0:T(1,128)} %bitcast.27, bf16[256,128]{1,0:T(8,128)(2,1)} %refs_0_.1, bf16[256,128]{1,0:T(8,128)(2,1)} %refs_1_.1, bf16[256,128]{1,0:T(8,128)(2,1)} %refs_2_.1, bf16[256,256]{1,0:T(8,128)(2,1)} %refs_3_.1, bf16[256,256]{1,0:T(8,128)(2,1)} %refs_4_.1), custom_call_target="tpu_custom_call" | custom-call | tf_op jit(solution)/shard_map/project/pallas_call | solution.py:62
  2.2 44.4 %all-to-all-start = ((bf16[16,8,1024]{2,1,0:T(8,128)(2,1)}), bf16[16,8,1024]{2,1,0:T(8,128)(2,1)S(1)}, u32[]{:S(2)}, u32[]{:S(2)}) async-start(bf16[16,8,1024]{2,1,0:T(8,128)(2,1)} %bitcast.25), calls=%async_computation | async-start | bytes 524288 | tf_op jit(solution)/shard_map/all_to_all | solution.py:23
  46.5 3.1 %collective-permute-start.1 = (bf16[256,1024]{1,0:T(8,128)(2,1)}, bf16[256,1024]{1,0:T(8,128)(2,1)}, u32[]{:S(2)}, u32[]{:S(2)}) collective-permute-start(bf16[256,1024]{1,0:T(8,128)(2,1)} %first.1), channel_id=1, source_target_pairs={{0,1},{1,0},{2,3},{3,2},{4,5},{5,4},{6,7},{7,6},{8,9},{9,8},{10,11... | collective-permute-start | bytes 1572872 | tf_op jit(solution)/shard_map/ppermute | solution.py:346
  49.6 2.0 %collective-permute-start.2 = (bf16[1024,256]{1,0:T(8,128)(2,1)}, bf16[1024,256]{1,0:T(8,128)(2,1)}, u32[]{:S(2)}, u32[]{:S(2)}) collective-permute-start(bf16[1024,256]{1,0:T(8,128)(2,1)} %param.35), channel_id=1, source_target_pairs={{0,1},{1,0},{2,3},{3,2},{4,5},{5,4},{6,7},{7,6},{8,9},{9,8},{10,11... | collective-permute-start | bytes 1572872 | tf_op jit(solution)/shard_map/ppermute | solution.py:347
  51.6 2.4 %collective-permute-start = (bf16[256,256]{1,0:T(8,128)(2,1)}, bf16[256,256]{1,0:T(8,128)(2,1)}, u32[]{:S(2)}, u32[]{:S(2)}) collective-permute-start(bf16[256,256]{1,0:T(8,128)(2,1)} %param.32), channel_id=1, source_target_pairs={{0,1},{1,0},{2,3},{3,2},{4,5},{5,4},{6,7},{7,6},{8,9},{9,8},{10,11... | collective-permute-start | bytes 393224 | tf_op jit(solution)/shard_map/ppermute | solution.py:345
  54.1 0.0 copy-start.7
  54.2 0.0 copy-start.5
  54.2 0.0 copy-start.6
  54.2 0.6 copy-done.7
  54.8 0.0 copy-done.8
  54.8 0.1 copy-done.5
  54.9 1.0 copy-done.2
  55.9 0.9 span.1
  56.8 0.0 copy-start.3
  56.8 1.0 broadcast_select_fusion
  57.9 2.2 %all-to-all-done.arrived = bf16[16,8,1024]{2,1,0:T(8,128)(2,1)S(1)} async-done(((bf16[16,8,1024]{2,1,0:T(8,128)(2,1)}), bf16[16,8,1024]{2,1,0:T(8,128)(2,1)S(1)}, u32[]{:S(2)}, u32[]{:S(2)}) %all-to-all-start) | async-done | bytes 262176 | tf_op jit(solution)/shard_map/all_to_all | solution.py:23
  60.1 1.6 attend.1
  61.7 24.2 %all_to_all.30 = bf16[32,4,256]{2,1,0:T(4,128)(2,1)S(1)} all-to-all(bf16[32,4,256]{2,1,0:T(4,128)(2,1)S(1)} %get-tuple-element.39), channel_id=1, replica_groups=mesh['grp'=2,'kv'=16,'x'=8,'core'=2] {'kv','core'}, dimensions={0} | all-to-all | bytes 131072 | tf_op jit(solution)/shard_map/all_to_all | solution.py:23
  86.0 0.0 copy-start.4
  86.0 0.2 merge.1
  86.2 16.2 %all_to_all.31.arrived = bf16[8,64,256]{2,1,0:T(8,128)(2,1)S(1)} all-to-all(bf16[8,64,256]{2,1,0:T(8,128)(2,1)S(1)} %merge.1), channel_id=1, replica_groups=mesh['grp'=2,'kv'=16,'x'=8,'core'=2] {'x'}, dimensions={0} | all-to-all | bytes 524288 | tf_op jit(solution)/shard_map/all_to_all | solution.py:23
  102.4 1.4 hidden.1
  103.7 15.6 %all_to_all.32.arrived = bf16[16,4,2176]{2,1,0:T(4,128)(2,1)S(1)} all-to-all(bf16[16,4,2176]{2,1,0:T(4,128)(2,1)S(1)} %get-tuple-element.47), channel_id=1, replica_groups=mesh['grp'=2,'kv'=16,'x'=8,'core'=2] {'kv'}, dimensions={0} | all-to-all | bytes 557056 | tf_op jit(solution)/shard_map/all_to_all | solution.py:23
  119.4 0.1 active.1
  119.5 18.9 %all_to_all.33 = bf16[16,4,2048]{2,1,0:T(4,128)(2,1)S(1)} all-to-all(bf16[16,4,2048]{2,1,0:T(4,128)(2,1)S(1)} %active.1), channel_id=1, replica_groups=mesh['grp'=2,'kv'=16,'x'=8,'core'=2] {'kv'}, dimensions={0} | all-to-all | bytes 524288 | tf_op jit(solution)/shard_map/all_to_all | solution.py:23
  138.5 0.1 reshape.46
  138.5 0.2 fusion.2
  138.7 0.2 fusion
  139.0 11.8 %all_to_all.34 = bf16[8,64,256]{2,1,0:T(8,128)(2,1)S(1)} all-to-all(bf16[8,64,256]{2,1,0:T(8,128)(2,1)S(1)} %broadcast_in_dim.2), channel_id=1, replica_groups=mesh['grp'=2,'kv'=16,'x'=8,'core'=2] {'x'}, dimensions={0} | all-to-all | bytes 524288 | tf_op jit(solution)/shard_map/all_to_all | solution.py:23
  150.8 13.8 %collective-permute-start.3 = (bf16[64,256]{1,0:T(8,128)(2,1)S(1)}, bf16[64,256]{1,0:T(8,128)(2,1)S(1)}, u32[]{:S(2)}, u32[]{:S(2)}) collective-permute-start(bf16[64,256]{1,0:T(8,128)(2,1)S(1)} %add_convert_fusion), channel_id=1, source_target_pairs={{0,1},{1,0},{2,3},{3,2},{4,5},{5,4},{6,7},{7,6},{8,9},{9,8},{10,11... | collective-permute-start | bytes 98312 | tf_op jit(solution)/shard_map/ppermute | solution.py:391
  164.7 0.8 collective-permute-done.3
  165.6 0.7 maximum_bitcast_fusion
  (28 shorter events, 0.3 us)
Async XLA Ops:
  0.0 54.2 %copy-start.1 = (f32[8,128,256]{2,1,0:T(8,128)S(1)}, f32[8,128,256]{2,1,0:T(8,128)}, u32[]{:S(2)}) copy-start(f32[8,128,256]{2,1,0:T(8,128)} %decays.1) | copy-start | bytes 3145732
  2.2 51.9 %copy-start.10 = (bf16[128,256]{1,0:T(8,128)(2,1)S(1)}, bf16[128,256]{1,0:T(8,128)(2,1)}, u32[]{:S(2)}) copy-start(bf16[128,256]{1,0:T(8,128)(2,1)} %tokens.1) | copy-start | bytes 196612
  2.2 57.9 %all-to-all-start = ((bf16[16,8,1024]{2,1,0:T(8,128)(2,1)}), bf16[16,8,1024]{2,1,0:T(8,128)(2,1)S(1)}, u32[]{:S(2)}, u32[]{:S(2)}) async-start(bf16[16,8,1024]{2,1,0:T(8,128)(2,1)} %bitcast.25), calls=%async_computation | async-start | bytes 524288 | tf_op jit(solution)/shard_map/all_to_all | solution.py:23
  46.5 11.3 %collective-permute-start.1 = (bf16[256,1024]{1,0:T(8,128)(2,1)}, bf16[256,1024]{1,0:T(8,128)(2,1)}, u32[]{:S(2)}, u32[]{:S(2)}) collective-permute-start(bf16[256,1024]{1,0:T(8,128)(2,1)} %first.1), channel_id=1, source_target_pairs={{0,1},{1,0},{2,3},{3,2},{4,5},{5,4},{6,7},{7,6},{8,9},{9,8},{10,11... | collective-permute-start | bytes 1572872 | tf_op jit(solution)/shard_map/ppermute | solution.py:346
  49.6 8.2 %collective-permute-start.2 = (bf16[1024,256]{1,0:T(8,128)(2,1)}, bf16[1024,256]{1,0:T(8,128)(2,1)}, u32[]{:S(2)}, u32[]{:S(2)}) collective-permute-start(bf16[1024,256]{1,0:T(8,128)(2,1)} %param.35), channel_id=1, source_target_pairs={{0,1},{1,0},{2,3},{3,2},{4,5},{5,4},{6,7},{7,6},{8,9},{9,8},{10,11... | collective-permute-start | bytes 1572872 | tf_op jit(solution)/shard_map/ppermute | solution.py:347
  51.6 5.2 %collective-permute-start = (bf16[256,256]{1,0:T(8,128)(2,1)}, bf16[256,256]{1,0:T(8,128)(2,1)}, u32[]{:S(2)}, u32[]{:S(2)}) collective-permute-start(bf16[256,256]{1,0:T(8,128)(2,1)} %param.32), channel_id=1, source_target_pairs={{0,1},{1,0},{2,3},{3,2},{4,5},{5,4},{6,7},{7,6},{8,9},{9,8},{10,11... | collective-permute-start | bytes 393224 | tf_op jit(solution)/shard_map/ppermute | solution.py:345
  54.1 0.7 copy-start.7
  54.1 0.7 copy-start.8
  54.2 0.7 copy-start.5
  54.2 0.7 copy-start.6
  54.9 1.0 copy-start.2
  55.9 4.2 %copy-start = (bf16[8,256,256]{2,1,0:T(8,128)(2,1)S(1)}, bf16[8,256,256]{2,1,0:T(8,128)(2,1)}, u32[]{:S(2)}) copy-start(bf16[8,256,256]{2,1,0:T(8,128)(2,1)} %values.1) | copy-start | bytes 3145732
  56.8 3.3 %copy-start.3 = (f32[8,4,32,64]{3,2,1,0:T(8,128)S(1)}, f32[8,4,32,64]{3,2,1,0:T(8,128)}, u32[]{:S(2)}) copy-start(f32[8,4,32,64]{3,2,1,0:T(8,128)} %state.1) | copy-start | bytes 786436
  86.0 16.4 %copy-start.4 = (bf16[256,1024]{1,0:T(8,128)(2,1)S(1)}, bf16[256,1024]{1,0:T(8,128)(2,1)}, u32[]{:S(2)}) copy-start(bf16[256,1024]{1,0:T(8,128)(2,1)} %first.1) | copy-start | bytes 1572868
  119.5 19.0 %copy-start.9 = (bf16[1024,256]{1,0:T(8,128)(2,1)S(1)}, bf16[1024,256]{1,0:T(8,128)(2,1)}, u32[]{:S(2)}) copy-start(bf16[1024,256]{1,0:T(8,128)(2,1)} %param.35) | copy-start | bytes 1572868
  150.8 14.7 %collective-permute-start.3 = (bf16[64,256]{1,0:T(8,128)(2,1)S(1)}, bf16[64,256]{1,0:T(8,128)(2,1)S(1)}, u32[]{:S(2)}, u32[]{:S(2)}) collective-permute-start(bf16[64,256]{1,0:T(8,128)(2,1)S(1)} %add_convert_fusion), channel_id=1, source_target_pairs={{0,1},{1,0},{2,3},{3,2},{4,5},{5,4},{6,7},{7,6},{8,9},{9,8},{10,11... | collective-permute-start | bytes 98312 | tf_op jit(solution)/shard_map/ppermute | solution.py:391

commit v7 on v6

--- a/solution.py
+++ b/solution.py
@@ -11,7 +11,7 @@
 LANES = 128
 SUBLANES = 8
 CORES = 2
-STAGGER_NS = 5600
+STAGGER_NS = 3500
 
 NORM_EPS = 1e-06
 DECAY_SOFTNESS = 16.0
@@ -184,8 +184,9 @@
     low = mixed.astype(bf16)
     for c in range(CORES):
         piece = low[c * half : (c + 1) * half]
-        for k in range(out.shape[0] // CORES):
-            out[k * CORES + c] = piece
+        pieces = out.shape[0] // CORES
+        for k in range(pieces):
+            out[c * pieces + k] = piece
     for copy in copies:
         copy.wait()
 
@@ -370,10 +371,10 @@
         gain,
         (out_first, out_second),
     )
-    heads = exchange(spread, ("kv", "core")).reshape(peers, CORES, half, values)
+    heads = exchange(spread, ("core", "kv")).reshape(CORES, rows_half, values)
     attn_terms = merge(
-        heads[:, 0].reshape(rows_half, values),
-        heads[:, 1].reshape(rows_half, values),
+        heads[0],
+        heads[1],
         out_first,
         out_second,
         lax.axis_size("x"),

time: 167 us -> 167 us (level)
  blocking collectives: 86.7 us -> 90.9 us
  starting transfers between devices: 65.7 us -> 62 us
    all_to_all x5, blocking collectives: 86.7 us -> 90.9 us  [exchange(): return lax.all_to_all(pieces, axes, 0, 0, tiled=True)]
    ppermute x1, starting transfers between devices: 13.8 us -> 10.1 us  [shards(): other_out = lax.ppermute(own_out, 'core', swap)]
where the time goes in v7:
time: 167 us
  blocking collectives  90.9 us (54%)
  starting transfers between devices  62 us (37%)
  Pallas kernels  6.31 us (4%)
  waiting for transfers between devices  3.07 us (2%)
  local copies, waits for them, and re-layouts  1.97 us (1%)
  other arithmetic  1.77 us (1%)
    all_to_all x5, blocking collectives, exchange(): return lax.all_to_all(pieces, axes, 0, 0, tiled=True)  90.9 us
    all_to_all x1, starting transfers between devices, exchange(): return lax.all_to_all(pieces, axes, 0, 0, tiled=True)  44.4 us
    ppermute x1, starting transfers between devices, shards(): other_out = lax.ppermute(own_out, 'core', swap)  10.1 us
  transfers between devices with their start and end apart: 5, of which 2 were waited for; matrix products, arithmetic and copies ran while one was open for 1% of the time, Pallas kernels for 1%

profile of v7, /device:TPU:65, one launch (start us, length us, event | category | flops | bytes accessed | tf_op | source)
XLA Modules:
  0.0 166.7 jit_solution(1377515030969269457)
XLA Ops:
  0.0 2.2 %project.1 = bf16[128,1024]{1,0:T(8,128)(2,1)} custom-call(bf16[128,256]{1,0:T(8,128)(2,1)} %tokens.1, f32[1,256]{1,0:T(1,128)} %bitcast.17, bf16[256,128]{1,0:T(8,128)(2,1)} %refs_0_.1, bf16[256,128]{1,0:T(8,128)(2,1)} %refs_1_.1, bf16[256,128]{1,0:T(8,128)(2,1)} %refs_2_.1, bf16[256,256]{1,0:T(8,128)(2,1)} %refs_3_.1, bf16[256,256]{1,0:T(8,128)(2,1)} %refs_4_.1), custom_call_target="tpu_custom_call" | custom-call | tf_op jit(solution)/shard_map/project/pallas_call | solution.py:62
  2.2 44.4 %all-to-all-start = ((bf16[16,8,1024]{2,1,0:T(8,128)(2,1)}), bf16[16,8,1024]{2,1,0:T(8,128)(2,1)S(1)}, u32[]{:S(2)}, u32[]{:S(2)}) async-start(bf16[16,8,1024]{2,1,0:T(8,128)(2,1)} %bitcast.16), calls=%async_computation | async-start | bytes 524288 | tf_op jit(solution)/shard_map/all_to_all | solution.py:23
  46.5 3.1 %collective-permute-start.1 = (bf16[256,1024]{1,0:T(8,128)(2,1)}, bf16[256,1024]{1,0:T(8,128)(2,1)}, u32[]{:S(2)}, u32[]{:S(2)}) collective-permute-start(bf16[256,1024]{1,0:T(8,128)(2,1)} %first.1), channel_id=1, source_target_pairs={{0,1},{1,0},{2,3},{3,2},{4,5},{5,4},{6,7},{7,6},{8,9},{9,8},{10,11... | collective-permute-start | bytes 1572872 | tf_op jit(solution)/shard_map/ppermute | solution.py:347
  49.6 2.0 %collective-permute-start.2 = (bf16[1024,256]{1,0:T(8,128)(2,1)}, bf16[1024,256]{1,0:T(8,128)(2,1)}, u32[]{:S(2)}, u32[]{:S(2)}) collective-permute-start(bf16[1024,256]{1,0:T(8,128)(2,1)} %param.35), channel_id=1, source_target_pairs={{0,1},{1,0},{2,3},{3,2},{4,5},{5,4},{6,7},{7,6},{8,9},{9,8},{10,11... | collective-permute-start | bytes 1572872 | tf_op jit(solution)/shard_map/ppermute | solution.py:348
  51.6 2.4 %collective-permute-start = (bf16[256,256]{1,0:T(8,128)(2,1)}, bf16[256,256]{1,0:T(8,128)(2,1)}, u32[]{:S(2)}, u32[]{:S(2)}) collective-permute-start(bf16[256,256]{1,0:T(8,128)(2,1)} %param.32), channel_id=1, source_target_pairs={{0,1},{1,0},{2,3},{3,2},{4,5},{5,4},{6,7},{7,6},{8,9},{9,8},{10,11... | collective-permute-start | bytes 393224 | tf_op jit(solution)/shard_map/ppermute | solution.py:346
  54.1 0.0 copy-start.8
  54.2 0.0 copy-start.6
  54.2 0.6 copy-done.7
  54.8 0.0 copy-done.8
  54.8 0.1 copy-done.5
  54.9 1.0 copy-done.2
  55.9 0.9 span.1
  56.8 0.0 copy-start.3
  56.8 1.0 broadcast_select_fusion
  57.9 2.2 %all-to-all-done.arrived = bf16[16,8,1024]{2,1,0:T(8,128)(2,1)S(1)} async-done(((bf16[16,8,1024]{2,1,0:T(8,128)(2,1)}), bf16[16,8,1024]{2,1,0:T(8,128)(2,1)S(1)}, u32[]{:S(2)}, u32[]{:S(2)}) %all-to-all-start) | async-done | bytes 262176 | tf_op jit(solution)/shard_map/all_to_all | solution.py:23
  60.1 1.6 attend.1
  61.7 25.0 %all_to_all.30 = bf16[32,4,256]{2,1,0:T(4,128)(2,1)S(1)} all-to-all(bf16[32,4,256]{2,1,0:T(4,128)(2,1)S(1)} %get-tuple-element.39), channel_id=1, replica_groups=mesh['grp'=2,'kv'=16,'x'=8,'core'=2] {'core','kv'}, dimensions={0} | all-to-all | bytes 131072 | tf_op jit(solution)/shard_map/all_to_all | solution.py:23
  86.8 0.0 copy-start.4
  86.8 0.2 merge.1
  87.0 16.3 %all_to_all.31.arrived = bf16[8,64,256]{2,1,0:T(8,128)(2,1)S(1)} all-to-all(bf16[8,64,256]{2,1,0:T(8,128)(2,1)S(1)} %merge.1), channel_id=1, replica_groups=mesh['grp'=2,'kv'=16,'x'=8,'core'=2] {'x'}, dimensions={0} | all-to-all | bytes 524288 | tf_op jit(solution)/shard_map/all_to_all | solution.py:23
  103.3 1.4 hidden.1
  104.7 15.6 %all_to_all.32.arrived = bf16[16,4,2176]{2,1,0:T(4,128)(2,1)S(1)} all-to-all(bf16[16,4,2176]{2,1,0:T(4,128)(2,1)S(1)} %get-tuple-element.47), channel_id=1, replica_groups=mesh['grp'=2,'kv'=16,'x'=8,'core'=2] {'kv'}, dimensions={0} | all-to-all | bytes 557056 | tf_op jit(solution)/shard_map/all_to_all | solution.py:23
  120.2 0.1 active.1
  120.4 0.0 copy-start.9
  120.4 22.3 %all_to_all.33 = bf16[16,4,2048]{2,1,0:T(4,128)(2,1)S(1)} all-to-all(bf16[16,4,2048]{2,1,0:T(4,128)(2,1)S(1)} %active.1), channel_id=1, replica_groups=mesh['grp'=2,'kv'=16,'x'=8,'core'=2] {'kv'}, dimensions={0} | all-to-all | bytes 524288 | tf_op jit(solution)/shard_map/all_to_all | solution.py:23
  142.6 0.1 reshape.47
  142.7 0.2 fusion.2
  142.9 0.2 fusion
  143.2 11.8 %all_to_all.34 = bf16[8,64,256]{2,1,0:T(8,128)(2,1)S(1)} all-to-all(bf16[8,64,256]{2,1,0:T(8,128)(2,1)S(1)} %broadcast_in_dim.2), channel_id=1, replica_groups=mesh['grp'=2,'kv'=16,'x'=8,'core'=2] {'x'}, dimensions={0} | all-to-all | bytes 524288 | tf_op jit(solution)/shard_map/all_to_all | solution.py:23
  155.0 10.1 %collective-permute-start.3 = (bf16[64,256]{1,0:T(8,128)(2,1)S(1)}, bf16[64,256]{1,0:T(8,128)(2,1)S(1)}, u32[]{:S(2)}, u32[]{:S(2)}) collective-permute-start(bf16[64,256]{1,0:T(8,128)(2,1)S(1)} %add_convert_fusion), channel_id=1, source_target_pairs={{0,1},{1,0},{2,3},{3,2},{4,5},{5,4},{6,7},{7,6},{8,9},{9,8},{10,11... | collective-permute-start | bytes 98312 | tf_op jit(solution)/shard_map/ppermute | solution.py:392
  165.1 0.8 collective-permute-done.3
  166.0 0.7 maximum_bitcast_fusion
  (28 shorter events, 0.3 us)
Async XLA Ops:
  0.0 54.2 %copy-start.1 = (f32[8,128,256]{2,1,0:T(8,128)S(1)}, f32[8,128,256]{2,1,0:T(8,128)}, u32[]{:S(2)}) copy-start(f32[8,128,256]{2,1,0:T(8,128)} %decays.1) | copy-start | bytes 3145732
  2.2 51.9 %copy-start.10 = (bf16[128,256]{1,0:T(8,128)(2,1)S(1)}, bf16[128,256]{1,0:T(8,128)(2,1)}, u32[]{:S(2)}) copy-start(bf16[128,256]{1,0:T(8,128)(2,1)} %tokens.1) | copy-start | bytes 196612
  2.2 57.9 %all-to-all-start = ((bf16[16,8,1024]{2,1,0:T(8,128)(2,1)}), bf16[16,8,1024]{2,1,0:T(8,128)(2,1)S(1)}, u32[]{:S(2)}, u32[]{:S(2)}) async-start(bf16[16,8,1024]{2,1,0:T(8,128)(2,1)} %bitcast.16), calls=%async_computation | async-start | bytes 524288 | tf_op jit(solution)/shard_map/all_to_all | solution.py:23
  46.5 11.3 %collective-permute-start.1 = (bf16[256,1024]{1,0:T(8,128)(2,1)}, bf16[256,1024]{1,0:T(8,128)(2,1)}, u32[]{:S(2)}, u32[]{:S(2)}) collective-permute-start(bf16[256,1024]{1,0:T(8,128)(2,1)} %first.1), channel_id=1, source_target_pairs={{0,1},{1,0},{2,3},{3,2},{4,5},{5,4},{6,7},{7,6},{8,9},{9,8},{10,11... | collective-permute-start | bytes 1572872 | tf_op jit(solution)/shard_map/ppermute | solution.py:347
  49.6 8.2 %collective-permute-start.2 = (bf16[1024,256]{1,0:T(8,128)(2,1)}, bf16[1024,256]{1,0:T(8,128)(2,1)}, u32[]{:S(2)}, u32[]{:S(2)}) collective-permute-start(bf16[1024,256]{1,0:T(8,128)(2,1)} %param.35), channel_id=1, source_target_pairs={{0,1},{1,0},{2,3},{3,2},{4,5},{5,4},{6,7},{7,6},{8,9},{9,8},{10,11... | collective-permute-start | bytes 1572872 | tf_op jit(solution)/shard_map/ppermute | solution.py:348
  51.6 5.2 %collective-permute-start = (bf16[256,256]{1,0:T(8,128)(2,1)}, bf16[256,256]{1,0:T(8,128)(2,1)}, u32[]{:S(2)}, u32[]{:S(2)}) collective-permute-start(bf16[256,256]{1,0:T(8,128)(2,1)} %param.32), channel_id=1, source_target_pairs={{0,1},{1,0},{2,3},{3,2},{4,5},{5,4},{6,7},{7,6},{8,9},{9,8},{10,11... | collective-permute-start | bytes 393224 | tf_op jit(solution)/shard_map/ppermute | solution.py:346
  54.1 0.7 copy-start.7
  54.1 0.7 copy-start.8
  54.2 0.7 copy-start.5
  54.2 0.7 copy-start.6
  54.9 1.0 copy-start.2
  55.9 4.2 %copy-start = (bf16[8,256,256]{2,1,0:T(8,128)(2,1)S(1)}, bf16[8,256,256]{2,1,0:T(8,128)(2,1)}, u32[]{:S(2)}) copy-start(bf16[8,256,256]{2,1,0:T(8,128)(2,1)} %values.1) | copy-start | bytes 3145732
  56.8 3.3 %copy-start.3 = (f32[8,4,32,64]{3,2,1,0:T(8,128)S(1)}, f32[8,4,32,64]{3,2,1,0:T(8,128)}, u32[]{:S(2)}) copy-start(f32[8,4,32,64]{3,2,1,0:T(8,128)} %state.1) | copy-start | bytes 786436
  86.8 16.5 %copy-start.4 = (bf16[256,1024]{1,0:T(8,128)(2,1)S(1)}, bf16[256,1024]{1,0:T(8,128)(2,1)}, u32[]{:S(2)}) copy-start(bf16[256,1024]{1,0:T(8,128)(2,1)} %first.1) | copy-start | bytes 1572868
  120.4 22.3 %copy-start.9 = (bf16[1024,256]{1,0:T(8,128)(2,1)S(1)}, bf16[1024,256]{1,0:T(8,128)(2,1)}, u32[]{:S(2)}) copy-start(bf16[1024,256]{1,0:T(8,128)(2,1)} %param.35) | copy-start | bytes 1572868
  155.0 10.9 %collective-permute-start.3 = (bf16[64,256]{1,0:T(8,128)(2,1)S(1)}, bf16[64,256]{1,0:T(8,128)(2,1)S(1)}, u32[]{:S(2)}, u32[]{:S(2)}) collective-permute-start(bf16[64,256]{1,0:T(8,128)(2,1)S(1)} %add_convert_fusion), channel_id=1, source_target_pairs={{0,1},{1,0},{2,3},{3,2},{4,5},{5,4},{6,7},{7,6},{8,9},{9,8},{10,11... | collective-permute-start | bytes 98312 | tf_op jit(solution)/shard_map/ppermute | solution.py:392

commit v8 on v7

--- a/solution.py
+++ b/solution.py
@@ -11,7 +11,7 @@
 LANES = 128
 SUBLANES = 8
 CORES = 2
-STAGGER_NS = 3500
+STAGGER_NS = 4500
 
 NORM_EPS = 1e-06
 DECAY_SOFTNESS = 16.0

time: 167 us -> 165 us (0.988)
  blocking collectives: 90.9 us -> 87.6 us
    all_to_all x5, blocking collectives: 90.9 us -> 87.6 us  [exchange(): return lax.all_to_all(pieces, axes, 0, 0, tiled=True)]
where the time goes in v8:
time: 165 us
  blocking collectives  87.6 us (53%)
  starting transfers between devices  63.1 us (38%)
  Pallas kernels  6.31 us (4%)
  waiting for transfers between devices  3.07 us (2%)
  local copies, waits for them, and re-layouts  1.97 us (1%)
  other arithmetic  1.77 us (1%)
    all_to_all x5, blocking collectives, exchange(): return lax.all_to_all(pieces, axes, 0, 0, tiled=True)  87.6 us
    all_to_all x1, starting transfers between devices, exchange(): return lax.all_to_all(pieces, axes, 0, 0, tiled=True)  44.4 us
    ppermute x1, starting transfers between devices, shards(): other_out = lax.ppermute(own_out, 'core', swap)  11.2 us
  transfers between devices with their start and end apart: 5, of which 2 were waited for; matrix products, arithmetic and copies ran while one was open for 1% of the time, Pallas kernels for 1%

profile of v8, /device:TPU:65, one launch (start us, length us, event | category | flops | bytes accessed | tf_op | source)
XLA Modules:
  0.0 164.5 jit_solution(1083769821571939353)
XLA Ops:
  0.0 2.2 %project.1 = bf16[128,1024]{1,0:T(8,128)(2,1)} custom-call(bf16[128,256]{1,0:T(8,128)(2,1)} %tokens.1, f32[1,256]{1,0:T(1,128)} %bitcast.17, bf16[256,128]{1,0:T(8,128)(2,1)} %refs_0_.1, bf16[256,128]{1,0:T(8,128)(2,1)} %refs_1_.1, bf16[256,128]{1,0:T(8,128)(2,1)} %refs_2_.1, bf16[256,256]{1,0:T(8,128)(2,1)} %refs_3_.1, bf16[256,256]{1,0:T(8,128)(2,1)} %refs_4_.1), custom_call_target="tpu_custom_call" | custom-call | tf_op jit(solution)/shard_map/project/pallas_call | solution.py:62
  2.2 44.4 %all-to-all-start = ((bf16[16,8,1024]{2,1,0:T(8,128)(2,1)}), bf16[16,8,1024]{2,1,0:T(8,128)(2,1)S(1)}, u32[]{:S(2)}, u32[]{:S(2)}) async-start(bf16[16,8,1024]{2,1,0:T(8,128)(2,1)} %bitcast.16), calls=%async_computation | async-start | bytes 524288 | tf_op jit(solution)/shard_map/all_to_all | solution.py:23
  46.5 3.1 %collective-permute-start.1 = (bf16[256,1024]{1,0:T(8,128)(2,1)}, bf16[256,1024]{1,0:T(8,128)(2,1)}, u32[]{:S(2)}, u32[]{:S(2)}) collective-permute-start(bf16[256,1024]{1,0:T(8,128)(2,1)} %first.1), channel_id=1, source_target_pairs={{0,1},{1,0},{2,3},{3,2},{4,5},{5,4},{6,7},{7,6},{8,9},{9,8},{10,11... | collective-permute-start | bytes 1572872 | tf_op jit(solution)/shard_map/ppermute | solution.py:347
  49.6 2.0 %collective-permute-start.2 = (bf16[1024,256]{1,0:T(8,128)(2,1)}, bf16[1024,256]{1,0:T(8,128)(2,1)}, u32[]{:S(2)}, u32[]{:S(2)}) collective-permute-start(bf16[1024,256]{1,0:T(8,128)(2,1)} %param.35), channel_id=1, source_target_pairs={{0,1},{1,0},{2,3},{3,2},{4,5},{5,4},{6,7},{7,6},{8,9},{9,8},{10,11... | collective-permute-start | bytes 1572872 | tf_op jit(solution)/shard_map/ppermute | solution.py:348
  51.6 2.4 %collective-permute-start = (bf16[256,256]{1,0:T(8,128)(2,1)}, bf16[256,256]{1,0:T(8,128)(2,1)}, u32[]{:S(2)}, u32[]{:S(2)}) collective-permute-start(bf16[256,256]{1,0:T(8,128)(2,1)} %param.32), channel_id=1, source_target_pairs={{0,1},{1,0},{2,3},{3,2},{4,5},{5,4},{6,7},{7,6},{8,9},{9,8},{10,11... | collective-permute-start | bytes 393224 | tf_op jit(solution)/shard_map/ppermute | solution.py:346
  54.1 0.0 copy-start.7
  54.1 0.0 copy-start.8
  54.2 0.0 copy-start.5
  54.2 0.0 copy-start.6
  54.2 0.6 copy-done.7
  54.8 0.0 copy-done.8
  54.8 0.1 copy-done.5
  54.9 1.0 copy-done.2
  55.9 0.9 span.1
  56.8 1.0 broadcast_select_fusion
  57.9 2.2 %all-to-all-done.arrived = bf16[16,8,1024]{2,1,0:T(8,128)(2,1)S(1)} async-done(((bf16[16,8,1024]{2,1,0:T(8,128)(2,1)}), bf16[16,8,1024]{2,1,0:T(8,128)(2,1)S(1)}, u32[]{:S(2)}, u32[]{:S(2)}) %all-to-all-start) | async-done | bytes 262176 | tf_op jit(solution)/shard_map/all_to_all | solution.py:23
  60.1 1.6 attend.1
  61.7 25.0 %all_to_all.30 = bf16[32,4,256]{2,1,0:T(4,128)(2,1)S(1)} all-to-all(bf16[32,4,256]{2,1,0:T(4,128)(2,1)S(1)} %get-tuple-element.39), channel_id=1, replica_groups=mesh['grp'=2,'kv'=16,'x'=8,'core'=2] {'core','kv'}, dimensions={0} | all-to-all | bytes 131072 | tf_op jit(solution)/shard_map/all_to_all | solution.py:23
  86.8 0.0 copy-start.4
  86.8 0.2 merge.1
  87.0 16.3 %all_to_all.31.arrived = bf16[8,64,256]{2,1,0:T(8,128)(2,1)S(1)} all-to-all(bf16[8,64,256]{2,1,0:T(8,128)(2,1)S(1)} %merge.1), channel_id=1, replica_groups=mesh['grp'=2,'kv'=16,'x'=8,'core'=2] {'x'}, dimensions={0} | all-to-all | bytes 524288 | tf_op jit(solution)/shard_map/all_to_all | solution.py:23
  103.2 1.4 hidden.1
  104.6 15.6 %all_to_all.32.arrived = bf16[16,4,2176]{2,1,0:T(4,128)(2,1)S(1)} all-to-all(bf16[16,4,2176]{2,1,0:T(4,128)(2,1)S(1)} %get-tuple-element.47), channel_id=1, replica_groups=mesh['grp'=2,'kv'=16,'x'=8,'core'=2] {'kv'}, dimensions={0} | all-to-all | bytes 557056 | tf_op jit(solution)/shard_map/all_to_all | solution.py:23
  120.2 0.1 active.1
  120.3 19.0 %all_to_all.33 = bf16[16,4,2048]{2,1,0:T(4,128)(2,1)S(1)} all-to-all(bf16[16,4,2048]{2,1,0:T(4,128)(2,1)S(1)} %active.1), channel_id=1, replica_groups=mesh['grp'=2,'kv'=16,'x'=8,'core'=2] {'kv'}, dimensions={0} | all-to-all | bytes 524288 | tf_op jit(solution)/shard_map/all_to_all | solution.py:23
  139.3 0.1 reshape.47
  139.4 0.2 fusion.2
  139.6 0.2 fusion
  139.9 11.8 %all_to_all.34 = bf16[8,64,256]{2,1,0:T(8,128)(2,1)S(1)} all-to-all(bf16[8,64,256]{2,1,0:T(8,128)(2,1)S(1)} %broadcast_in_dim.2), channel_id=1, replica_groups=mesh['grp'=2,'kv'=16,'x'=8,'core'=2] {'x'}, dimensions={0} | all-to-all | bytes 524288 | tf_op jit(solution)/shard_map/all_to_all | solution.py:23
  151.7 11.2 %collective-permute-start.3 = (bf16[64,256]{1,0:T(8,128)(2,1)S(1)}, bf16[64,256]{1,0:T(8,128)(2,1)S(1)}, u32[]{:S(2)}, u32[]{:S(2)}) collective-permute-start(bf16[64,256]{1,0:T(8,128)(2,1)S(1)} %add_convert_fusion), channel_id=1, source_target_pairs={{0,1},{1,0},{2,3},{3,2},{4,5},{5,4},{6,7},{7,6},{8,9},{9,8},{10,11... | collective-permute-start | bytes 98312 | tf_op jit(solution)/shard_map/ppermute | solution.py:392
  163.0 0.8 collective-permute-done.3
  163.8 0.7 maximum_bitcast_fusion
  (28 shorter events, 0.3 us)
Async XLA Ops:
  0.0 54.2 %copy-start.1 = (f32[8,128,256]{2,1,0:T(8,128)S(1)}, f32[8,128,256]{2,1,0:T(8,128)}, u32[]{:S(2)}) copy-start(f32[8,128,256]{2,1,0:T(8,128)} %decays.1) | copy-start | bytes 3145732
  2.2 51.9 %copy-start.10 = (bf16[128,256]{1,0:T(8,128)(2,1)S(1)}, bf16[128,256]{1,0:T(8,128)(2,1)}, u32[]{:S(2)}) copy-start(bf16[128,256]{1,0:T(8,128)(2,1)} %tokens.1) | copy-start | bytes 196612
  2.2 57.9 %all-to-all-start = ((bf16[16,8,1024]{2,1,0:T(8,128)(2,1)}), bf16[16,8,1024]{2,1,0:T(8,128)(2,1)S(1)}, u32[]{:S(2)}, u32[]{:S(2)}) async-start(bf16[16,8,1024]{2,1,0:T(8,128)(2,1)} %bitcast.16), calls=%async_computation | async-start | bytes 524288 | tf_op jit(solution)/shard_map/all_to_all | solution.py:23
  46.5 11.3 %collective-permute-start.1 = (bf16[256,1024]{1,0:T(8,128)(2,1)}, bf16[256,1024]{1,0:T(8,128)(2,1)}, u32[]{:S(2)}, u32[]{:S(2)}) collective-permute-start(bf16[256,1024]{1,0:T(8,128)(2,1)} %first.1), channel_id=1, source_target_pairs={{0,1},{1,0},{2,3},{3,2},{4,5},{5,4},{6,7},{7,6},{8,9},{9,8},{10,11... | collective-permute-start | bytes 1572872 | tf_op jit(solution)/shard_map/ppermute | solution.py:347
  49.6 8.2 %collective-permute-start.2 = (bf16[1024,256]{1,0:T(8,128)(2,1)}, bf16[1024,256]{1,0:T(8,128)(2,1)}, u32[]{:S(2)}, u32[]{:S(2)}) collective-permute-start(bf16[1024,256]{1,0:T(8,128)(2,1)} %param.35), channel_id=1, source_target_pairs={{0,1},{1,0},{2,3},{3,2},{4,5},{5,4},{6,7},{7,6},{8,9},{9,8},{10,11... | collective-permute-start | bytes 1572872 | tf_op jit(solution)/shard_map/ppermute | solution.py:348
  51.6 5.2 %collective-permute-start = (bf16[256,256]{1,0:T(8,128)(2,1)}, bf16[256,256]{1,0:T(8,128)(2,1)}, u32[]{:S(2)}, u32[]{:S(2)}) collective-permute-start(bf16[256,256]{1,0:T(8,128)(2,1)} %param.32), channel_id=1, source_target_pairs={{0,1},{1,0},{2,3},{3,2},{4,5},{5,4},{6,7},{7,6},{8,9},{9,8},{10,11... | collective-permute-start | bytes 393224 | tf_op jit(solution)/shard_map/ppermute | solution.py:346
  54.1 0.7 copy-start.7
  54.1 0.7 copy-start.8
  54.2 0.7 copy-start.5
  54.2 0.7 copy-start.6
  54.9 1.0 copy-start.2
  55.9 4.2 %copy-start = (bf16[8,256,256]{2,1,0:T(8,128)(2,1)S(1)}, bf16[8,256,256]{2,1,0:T(8,128)(2,1)}, u32[]{:S(2)}) copy-start(bf16[8,256,256]{2,1,0:T(8,128)(2,1)} %values.1) | copy-start | bytes 3145732
  56.8 3.3 %copy-start.3 = (f32[8,4,32,64]{3,2,1,0:T(8,128)S(1)}, f32[8,4,32,64]{3,2,1,0:T(8,128)}, u32[]{:S(2)}) copy-start(f32[8,4,32,64]{3,2,1,0:T(8,128)} %state.1) | copy-start | bytes 786436
  86.8 16.5 %copy-start.4 = (bf16[256,1024]{1,0:T(8,128)(2,1)S(1)}, bf16[256,1024]{1,0:T(8,128)(2,1)}, u32[]{:S(2)}) copy-start(bf16[256,1024]{1,0:T(8,128)(2,1)} %first.1) | copy-start | bytes 1572868
  120.3 19.1 %copy-start.9 = (bf16[1024,256]{1,0:T(8,128)(2,1)S(1)}, bf16[1024,256]{1,0:T(8,128)(2,1)}, u32[]{:S(2)}) copy-start(bf16[1024,256]{1,0:T(8,128)(2,1)} %param.35) | copy-start | bytes 1572868
  151.7 12.1 %collective-permute-start.3 = (bf16[64,256]{1,0:T(8,128)(2,1)S(1)}, bf16[64,256]{1,0:T(8,128)(2,1)S(1)}, u32[]{:S(2)}, u32[]{:S(2)}) collective-permute-start(bf16[64,256]{1,0:T(8,128)(2,1)S(1)} %add_convert_fusion), channel_id=1, source_target_pairs={{0,1},{1,0},{2,3},{3,2},{4,5},{5,4},{6,7},{7,6},{8,9},{9,8},{10,11... | collective-permute-start | bytes 98312 | tf_op jit(solution)/shard_map/ppermute | solution.py:392
